TPU v7x, 128 devices: a whole 4x4x4 slice. The times are simulated.
128 devices in a mesh: sp: 64 (over z, y, x), tp: 2 (over core).
Axes of the slice: x: 4, y: 4, z: 4, core: 2. Of those that a mesh axis runs over, the one named last changes fastest.
Arguments:
- residual: bfloat16 [16384, 2048], P(('sp', 'tp')), as said below
- outer_gate: bfloat16 [16384, 1024], P('sp', 'tp'), may hold values from -6 to 6
- conv_input: bfloat16 [16384, 1024], P('sp', 'tp'), as said below
- conv_value: bfloat16 [16384, 1024], P('sp', 'tp'), may hold values from -6 to 6
- doc_ids: int32 [16384], P('sp'), may hold values from 0 to 31, never falling along the last dimension, each value on 1 to 1024 neighbouring positions
- conv_taps: bfloat16 [3, 1024], P(None, 'tp'), may hold values from -3.5 to 3.5
- branch_gain: bfloat16 [1024], P('tp'), may hold values from 0.099609375 to 1.8984375
- out_weight: bfloat16 [1024, 2048], replicated, may hold values from -0.1875 to 0.1875
- ffn_gain: bfloat16 [2048], replicated, may hold values from 0.099609375 to 1.8984375
- route_ids: int32 [16384, 4], P(('sp', 'tp')), may hold values from 0 to 127, all different within a row; in each aligned block of 128 rows (0 to 127, 128 to 255, ...) at most 8 rows name the same one
- route_weight: float32 [16384, 4], P(('sp', 'tp')), may hold values from 0.2 to 1
- shared_gate: bfloat16 [2048, 512], replicated, may hold values from -0.125 to 0.125
- shared_up: bfloat16 [2048, 512], replicated, may hold values from -0.125 to 0.125
- shared_down: bfloat16 [512, 2048], replicated, may hold values from -0.25 to 0.25
- expert_gate: bfloat16 [128, 2048, 512], P(('sp', 'tp')), may hold values from -0.125 to 0.125
- expert_up: bfloat16 [128, 2048, 512], P(('sp', 'tp')), may hold values from -0.125 to 0.125
- expert_down: bfloat16 [128, 512, 2048], P(('sp', 'tp')), may hold values from -0.25 to 0.25
Outputs:
- layer_out: bfloat16 [16384, 2048], P(('sp', 'tp'))
Inputs may be any that keep to these rules, and one draw needn't show every extreme that they name: `route_ids`: each row names 4 different experts. Within each aligned block of 128 rows (the rows of one device) no expert is named by more than 8 rows, and in every draw some expert is named by exactly 8 rows of some block. `doc_ids`: document numbers start at 0 and never fall along the sequence; each document has 1 to 1024 positions. `residual`: Real-valued, of order one. `conv_input`: Real-valued, of order one.
All inputs are finite; a program needn't handle non-finite values.
Results may differ from a plain program's by a relative error of at most 0.012.
Values may be sent and summed in bfloat16 or wider, within the bound.
No kernel may reach another device: no remote copies, remote signals or barrier semaphores. Data moves between devices by JAX's collectives and lax.ppermute only.
A program may use at most 128 MiB of HBM per device.

v0:
```python
import jax
import jax.numpy as jnp
from jax import lax
from jax.sharding import PartitionSpec as P

norm_eps = 1e-06


def from_behind(value, axis, by):
    peers = lax.axis_size(axis)
    pairs = [(i, i + by) for i in range(peers) if 0 <= i + by < peers]
    return lax.ppermute(value, axis, pairs)


def total_of_pieces(value, axis):
    pieces = lax.all_gather(value, axis)
    return pieces.sum(axis=0)


def expert_apply(arrived, gate_w, up_w, down_w):
    flat_rows = arrived.reshape(-1, arrived.shape[-1])
    hidden = (
        jax.nn.silu(jnp.dot(flat_rows, gate_w, preferred_element_type=jnp.float32))
        * jnp.dot(flat_rows, up_w, preferred_element_type=jnp.float32)
    ).astype(jnp.bfloat16)
    result = jnp.dot(hidden, down_w, preferred_element_type=jnp.float32).astype(jnp.bfloat16)
    return result.reshape(arrived.shape)


def shards(
    residual,
    outer_gate,
    conv_input,
    conv_value,
    doc_ids,
    conv_taps,
    branch_gain,
    out_weight,
    ffn_gain,
    route_ids,
    route_weight,
    shared_gate,
    shared_up,
    shared_down,
    expert_gate,
    expert_up,
    expert_down,
):
    seq_rows = conv_input.shape[0]
    half_width = conv_input.shape[1]
    tap_count = conv_taps.shape[0]
    lead_rows = tap_count - 1
    doc_float = doc_ids.astype(jnp.float32)
    prev_input, prev_value, prev_doc = from_behind(
        (
            conv_input[seq_rows - lead_rows :],
            conv_value[seq_rows - lead_rows :],
            doc_float[seq_rows - lead_rows :].astype(jnp.bfloat16),
        ),
        "sp",
        1,
    )
    source = jnp.concatenate(
        [
            prev_input.astype(jnp.float32) * prev_value.astype(jnp.float32),
            conv_input.astype(jnp.float32) * conv_value.astype(jnp.float32),
        ],
        axis=0,
    )
    doc_extended = jnp.concatenate([prev_doc.astype(jnp.float32), doc_float], axis=0)
    mixed_conv = jnp.zeros((seq_rows, half_width), jnp.float32)
    for tap in range(tap_count):
        same_doc = (doc_extended[tap : tap + seq_rows] == doc_float).astype(jnp.float32)[:, None]
        mixed_conv = (
            mixed_conv
            + conv_taps[tap].astype(jnp.float32)[None, :] * source[tap : tap + seq_rows] * same_doc
        )
    branch = outer_gate.astype(jnp.float32) * mixed_conv
    square_total = total_of_pieces(jnp.sum(branch * branch, axis=1, keepdims=True), "tp")
    inv_rms = lax.rsqrt(square_total / (half_width * lax.axis_size("tp")) + norm_eps)
    normed = (branch * inv_rms * branch_gain.astype(jnp.float32)[None, :]).astype(jnp.bfloat16)
    local_rows = residual.shape[0]
    token_rows = lax.all_to_all(normed, "tp", split_axis=0, concat_axis=1, tiled=True)
    update = jnp.dot(token_rows, out_weight, preferred_element_type=jnp.float32)
    middle = (residual.astype(jnp.float32) + update).astype(jnp.bfloat16)
    mid_float = middle.astype(jnp.float32)
    mid_rms = lax.rsqrt(jnp.mean(mid_float * mid_float, axis=1, keepdims=True) + norm_eps)
    ffn_in = (mid_float * mid_rms * ffn_gain.astype(jnp.float32)[None, :]).astype(jnp.bfloat16)
    shared_hidden = (
        jax.nn.silu(jnp.dot(ffn_in, shared_gate, preferred_element_type=jnp.float32))
        * jnp.dot(ffn_in, shared_up, preferred_element_type=jnp.float32)
    ).astype(jnp.bfloat16)
    shared_out = jnp.dot(shared_hidden, shared_down, preferred_element_type=jnp.float32)
    model_width = residual.shape[1]
    top_count = route_ids.shape[1]
    seq_devices = lax.axis_size("sp")
    core_devices = lax.axis_size("tp")
    expert_count = seq_devices * core_devices
    capacity = local_rows * core_devices * top_count // expert_count
    flat_expert = route_ids.reshape(-1)
    onehot = (flat_expert[:, None] == jnp.arange(expert_count, dtype=jnp.int32)[None, :]).astype(
        jnp.int32
    )
    slot_rank = jnp.sum(onehot * (jnp.cumsum(onehot, axis=0) - onehot), axis=1)
    slot_of = flat_expert * capacity + slot_rank
    token_index = jnp.arange(local_rows * top_count, dtype=jnp.int32) // top_count
    slot_source = (
        jnp.full((expert_count * capacity,), local_rows, jnp.int32).at[slot_of].set(token_index)
    )
    padded_in = jnp.concatenate([ffn_in, jnp.zeros((1, model_width), jnp.bfloat16)], axis=0)
    outgoing = padded_in[slot_source].reshape(expert_count, capacity, model_width)
    gate_w = expert_gate[0]
    up_w = expert_up[0]
    down_w = expert_down[0]
    result = expert_apply(
        lax.all_to_all(outgoing, ("sp", "tp"), split_axis=0, concat_axis=0, tiled=True),
        gate_w,
        up_w,
        down_w,
    )
    returned = lax.all_to_all(result, ("sp", "tp"), split_axis=0, concat_axis=0, tiled=True)
    returned_rows = returned.reshape(expert_count * capacity, model_width)[slot_of]
    weighted = (
        returned_rows.astype(jnp.float32).reshape(local_rows, top_count, model_width)
        * route_weight[:, :, None]
    )
    routed = jnp.sum(weighted, axis=1)
    return (mid_float + shared_out + routed).astype(jnp.bfloat16)


def solution(mesh):
    placed = (
        P(("sp", "tp"), None),
        P("sp", "tp"),
        P("sp", "tp"),
        P("sp", "tp"),
        P("sp"),
        P(None, "tp"),
        P("tp"),
        P(),
        P(),
        P(("sp", "tp"), None),
        P(("sp", "tp"), None),
        P(),
        P(),
        P(),
        P(("sp", "tp"), None, None),
        P(("sp", "tp"), None, None),
        P(("sp", "tp"), None, None),
    )
    return jax.shard_map(
        shards, mesh=mesh, in_specs=placed, out_specs=P(("sp", "tp"), None), check_vma=False
    )
```

profile of v0, /device:TPU:1, one launch (start us, length us, event | category | flops | bytes accessed | tf_op | source)
XLA Modules:
  0.0 199.2 jit_solution(1361427338525140731)
XLA Ops:
  0.0 0.8 convert_convert_fusion
  0.9 3.9 %collective-permute-start.2 = (bf16[2]{0:T(256)(128)(2,1)S(1)}, bf16[2]{0:T(256)(128)(2,1)S(1)}, u32[]{:S(2)}, u32[]{:S(2)}) collective-permute-start(bf16[2]{0:T(256)(128)(2,1)S(1)} %slice.41), channel_id=1, source_target_pairs={{0,2},{2,4},{4,6},{6,8},{8,10},{10,12},{12,14},{14,16},{16,18},{18... | collective-permute-start | bytes 20 | tf_op jit(solution)/shard_map/ppermute | solution.py:12
  5.6 3.1 %collective-permute-start = (bf16[2,512]{1,0:T(2,128)(2,1)S(1)}, bf16[2,512]{1,0:T(2,128)(2,1)S(1)}, u32[]{:S(2)}, u32[]{:S(2)}) collective-permute-start(bf16[2,512]{1,0:T(2,128)(2,1)S(1)} %slice.38), channel_id=1, source_target_pairs={{0,2},{2,4},{4,6},{6,8},{8,10},{10,12},{12,14},{14,16},{16,18},{18... | collective-permute-start | bytes 6152 | tf_op jit(solution)/shard_map/ppermute | solution.py:12
  9.4 2.8 %collective-permute-start.1 = (bf16[2,512]{1,0:T(2,128)(2,1)S(1)}, bf16[2,512]{1,0:T(2,128)(2,1)S(1)}, u32[]{:S(2)}, u32[]{:S(2)}) collective-permute-start(bf16[2,512]{1,0:T(2,128)(2,1)S(1)} %slice.39), channel_id=1, source_target_pairs={{0,2},{2,4},{4,6},{6,8},{8,10},{10,12},{12,14},{14,16},{16,18},{18... | collective-permute-start | bytes 6152 | tf_op jit(solution)/shard_map/ppermute | solution.py:12
  12.2 1.1 convert_multiply_fusion
  13.3 0.8 copy.34
  15.0 0.8 slice_convert_fusion.2
  18.1 2.4 %scatter_custom_fusion = s32[1024]{0:T(1024)S(1)} fusion(s32[512]{0:T(512)S(1)} %bitcast.63, s32[512]{0:T(512)S(1)} %add_select_fusion, s32[]{:T(128)} %constant.42.clone.1), kind=kCustom, calls=%fused_computation.66 | custom fusion | bytes 4100 | tf_op jit(solution)/shard_map/scatter | solution.py:108
  21.1 3.0 %all-gather.1 = f32[2,1,256]{2,1,0:T(1,128)S(1)} all-gather(f32[1,1,256]{2,1,0:T(1,128)S(1)} %bitcast.68), channel_id=2, replica_groups=mesh['sp'=64,'tp'=2] {'tp'}, dimensions={0}, use_global_device_ids=true | all-gather | bytes 3072 | tf_op jit(solution)/shard_map/all_gather | solution.py:16
  24.3 3.9 %all_to_all.29 = bf16[2,128,512]{2,1,0:T(8,128)(2,1)S(1)} all-to-all(bf16[2,128,512]{2,1,0:T(8,128)(2,1)S(1)} %bitcast.58), channel_id=1, replica_groups=mesh['sp'=64,'tp'=2] {'tp'}, dimensions={0} | all-to-all | bytes 524288 | tf_op jit(solution)/shard_map/all_to_all | solution.py:83
  28.4 3.1 %multiply_reduce_fusion.1 = (f32[128]{0:T(128)S(1)}, f32[128,2048]{1,0:T(8,128)S(1)}) fusion(bf16[128,1024]{0,1:T(8,128)(2,1)S(1)} %bitcast.57, bf16[1024,2048]{1,0:T(8,128)(2,1)} %param.24, bf16[128,2048]{1,0:T(8,128)(2,1)} %param.17), kind=kOutput, calls=%fused_computation.23 | convolution fusion | flops 538443648 | bytes 6029824 | tf_op jit(solution)/shard_map/dot_general | solution.py:84
  31.5 1.0 copy-done.1
  32.7 6.0 %gather_fusion = bf16[1024,2048]{1,0:T(8,128)(2,1)} fusion(bf16[129,2048]{1,0:T(8,128)(2,1)S(1)} %concatenate.11, s32[1024]{0:T(1024)S(1)} %fusion.40), kind=kCustom, calls=%fused_computation | custom fusion | bytes 8392704 | tf_op jit(solution)/shard_map/gather | solution.py:111
  38.7 63.0 %all_to_all.30 = bf16[128,8,2048]{2,1,0:T(8,128)(2,1)S(1)} all-to-all(bf16[128,8,2048]{2,1,0:T(8,128)(2,1)} %bitcast.55), channel_id=1, replica_groups=mesh['sp'=64,'tp'=2] {'sp','tp'}, dimensions={0} | all-to-all | bytes 8388608 | tf_op jit(solution)/shard_map/all_to_all | solution.py:116
  101.8 2.0 copy-done.4
  103.7 3.7 %fusion.2 = f32[1024,512]{1,0:T(8,128)} fusion(bf16[128,8,2048]{2,1,0:T(8,128)(2,1)S(1)} %all_to_all.30, bf16[1,2048,512]{2,1,0:T(8,128)(2,1)S(1)} %copy-done.8), kind=kOutput, calls=%fused_computation.5 | convolution fusion | flops 2147483648 | bytes 8388608 | tf_op jit(solution)/shard_map/dot_general | solution.py:23
  107.5 10.0 %convert_bitcast_fusion = bf16[128,8,2048]{2,1,0:T(8,128)(2,1)} fusion(bf16[1,512,2048]{2,1,0:T(8,128)(2,1)S(1)} %copy-done, f32[1024,512]{1,0:T(8,128)} %fusion.2, bf16[1,2048,512]{2,1,0:T(8,128)(2,1)} %param.32, bf16[128,8,2048]{2,1,0:T(8,128)(2,1)} %copy-done.4), kind=kOutput, calls=%fused_computation.8 | convolution fusion | flops 4300210176 | bytes 14680064 | tf_op jit(solution)/shard_map/dot_general | solution.py:26
  117.4 5.7 %all-to-all-start.2 = ((bf16[128,8,2048]{2,1,0:T(8,128)(2,1)}), bf16[128,8,2048]{2,1,0:T(8,128)(2,1)}, u32[]{:S(2)}, u32[]{:S(2)}) async-start(bf16[128,8,2048]{2,1,0:T(8,128)(2,1)} %convert_bitcast_fusion), calls=%async_computation.2 | async-start | bytes 8388608 | tf_op jit(solution)/shard_map/all_to_all | solution.py:121
  123.2 2.0 %fusion.49 = f32[128,512]{1,0:T(8,128)S(1)} fusion(bf16[128,2048]{1,0:T(8,128)(2,1)S(1)} %multiply_convert_fusion.1, bf16[2048,512]{1,0:T(8,128)(2,1)} %param.28), kind=kOutput, calls=%fused_computation.81 | convolution fusion | flops 268435456 | bytes 2883584 | tf_op jit(solution)/shard_map/dot_general | solution.py:90
  125.3 50.5 %all-to-all-done.2 = bf16[128,8,2048]{2,1,0:T(8,128)(2,1)} async-done(((bf16[128,8,2048]{2,1,0:T(8,128)(2,1)}), bf16[128,8,2048]{2,1,0:T(8,128)(2,1)}, u32[]{:S(2)}, u32[]{:S(2)}) %all-to-all-start.2) | async-done | bytes 4194336 | tf_op jit(solution)/shard_map/all_to_all | solution.py:121
  175.8 8.0 %gather_fusion.1 = bf16[512,2048]{1,0:T(8,128)(2,1)} fusion(bf16[1024,2048]{1,0:T(8,128)(2,1)} %bitcast.18, s32[1024]{0:T(1024)S(1)} %pad_clamp_fusion), kind=kCustom, calls=%fused_computation.1 | custom fusion | bytes 4196352 | tf_op jit(solution)/shard_map/gather | solution.py:122
  183.8 4.8 %reshape.96 = f32[128,4,2048]{2,1,0:T(4,128)} reshape(bf16[512,2048]{1,0:T(8,128)(2,1)} %gather_fusion.1) | data formatting | bytes 6291456 | tf_op jit(solution)/shard_map/convert_element_type | solution.py:124
  188.5 6.4 %multiply_reduce_fusion = f32[128,2048]{1,0:T(8,128)} fusion(f32[128,4,2048]{2,1,0:T(4,128)} %reshape.96, f32[128,4]{1,0:T(8,128)S(1)} %copy.38), kind=kLoop, calls=%fused_computation.7 | loop fusion | flops 1835008 | bytes 5244928 | tf_op jit(solution)/shard_map/reduce_sum | solution.py:127
  194.9 4.3 %fusion.7 = bf16[128,2048]{1,0:T(8,128)(2,1)} fusion(f32[128,2048]{1,0:T(8,128)} %multiply_reduce_fusion, f32[128,2048]{1,0:T(8,128)S(1)} %copy-done.2, bf16[512,2048]{1,0:T(8,128)(2,1)} %param.30, bf16[128,2048]{1,0:T(8,128)(2,1)} %copy-done.3, bf16[2048,512]{1,0:T(8,128)(2,1)} %param.29, f32[128,512]{1,0:T(8,128)S(1)} %fusion.49), kind=kOutput, calls=%fused_computation.14 | convolution fusion | flops 538050560 | bytes 7602176 | tf_op jit(solution)/shard_map/dot_general | solution.py:93
  (55 shorter events, 5.9 us)
Async XLA Ops:
  0.0 107.5 %copy-start = (bf16[1,512,2048]{2,1,0:T(8,128)(2,1)S(1)}, bf16[1,512,2048]{2,1,0:T(8,128)(2,1)}, u32[]{:S(2)}) copy-start(bf16[1,512,2048]{2,1,0:T(8,128)(2,1)} %param.33) | copy-start | bytes 6291460
  0.0 20.6 %copy-start.6 = (s32[256]{0:T(256)S(1)}, s32[256]{0:T(256)}, u32[]{:S(2)}) copy-start(s32[256]{0:T(256)} %param.21) | copy-start | bytes 3076
  0.0 20.7 %copy-start.5 = (bf16[256,512]{1,0:T(8,128)(2,1)S(1)}, bf16[256,512]{1,0:T(8,128)(2,1)}, u32[]{:S(2)}) copy-start(bf16[256,512]{1,0:T(8,128)(2,1)} %param.18) | copy-start | bytes 786436
  0.9 19.6 %collective-permute-start.2 = (bf16[2]{0:T(256)(128)(2,1)S(1)}, bf16[2]{0:T(256)(128)(2,1)S(1)}, u32[]{:S(2)}, u32[]{:S(2)}) collective-permute-start(bf16[2]{0:T(256)(128)(2,1)S(1)} %slice.41), channel_id=1, source_target_pairs={{0,2},{2,4},{4,6},{6,8},{8,10},{10,12},{12,14},{14,16},{16,18},{18... | collective-permute-start | bytes 20 | tf_op jit(solution)/shard_map/ppermute | solution.py:12
  5.6 15.2 %collective-permute-start = (bf16[2,512]{1,0:T(2,128)(2,1)S(1)}, bf16[2,512]{1,0:T(2,128)(2,1)S(1)}, u32[]{:S(2)}, u32[]{:S(2)}) collective-permute-start(bf16[2,512]{1,0:T(2,128)(2,1)S(1)} %slice.38), channel_id=1, source_target_pairs={{0,2},{2,4},{4,6},{6,8},{8,10},{10,12},{12,14},{14,16},{16,18},{18... | collective-permute-start | bytes 6152 | tf_op jit(solution)/shard_map/ppermute | solution.py:12
  9.4 11.3 %collective-permute-start.1 = (bf16[2,512]{1,0:T(2,128)(2,1)S(1)}, bf16[2,512]{1,0:T(2,128)(2,1)S(1)}, u32[]{:S(2)}, u32[]{:S(2)}) collective-permute-start(bf16[2,512]{1,0:T(2,128)(2,1)S(1)} %slice.39), channel_id=1, source_target_pairs={{0,2},{2,4},{4,6},{6,8},{8,10},{10,12},{12,14},{14,16},{16,18},{18... | collective-permute-start | bytes 6152 | tf_op jit(solution)/shard_map/ppermute | solution.py:12
  31.5 1.0 copy-start.1
  32.6 90.6 %copy-start.3 = (bf16[128,2048]{1,0:T(8,128)(2,1)}, bf16[128,2048]{1,0:T(8,128)(2,1)S(1)}, u32[]{:S(2)}) copy-start(bf16[128,2048]{1,0:T(8,128)(2,1)S(1)} %multiply_convert_fusion.1) | copy-start | bytes 1572868
  38.7 65.0 %copy-start.8 = (bf16[1,2048,512]{2,1,0:T(8,128)(2,1)S(1)}, bf16[1,2048,512]{2,1,0:T(8,128)(2,1)}, u32[]{:S(2)}) copy-start(bf16[1,2048,512]{2,1,0:T(8,128)(2,1)} %param.31) | copy-start | bytes 6291460
  101.8 2.0 copy-start.4
  117.4 5.7 %copy-start.7 = (f32[128,4]{0,1:T(4,128)S(1)}, f32[128,4]{0,1:T(4,128)}, u32[]{:S(2)}) copy-start(f32[128,4]{0,1:T(4,128)} %param.27) | copy-start | bytes 6148
  117.4 58.4 %all-to-all-start.2 = ((bf16[128,8,2048]{2,1,0:T(8,128)(2,1)}), bf16[128,8,2048]{2,1,0:T(8,128)(2,1)}, u32[]{:S(2)}, u32[]{:S(2)}) async-start(bf16[128,8,2048]{2,1,0:T(8,128)(2,1)} %convert_bitcast_fusion), calls=%async_computation.2 | async-start | bytes 8388608 | tf_op jit(solution)/shard_map/all_to_all | solution.py:121
  188.5 6.4 %copy-start.2 = (f32[128,2048]{1,0:T(8,128)S(1)}, f32[128,2048]{1,0:T(8,128)}, u32[]{:S(2)}) copy-start(f32[128,2048]{1,0:T(8,128)} %copy-done.1) | copy-start | bytes 3145732
where the time goes:
time: 200 us; the launch traced here: 199 us
  blocking collectives  69.9 us (35%)
  waiting for transfers between devices  50.5 us (25%)
  local copies, waits for them, and re-layouts  27.3 us (14%)
  matrix products  23.1 us (12%)
  starting transfers between devices  15.5 us (8%)
  other arithmetic  12.6 us (6%)
    all_to_all x1, blocking collectives, shards(): lax.all_to_all(outgoing, ('sp', 'tp'), split_axis=0, concat_axis=0, tiled...  63 us
    all_to_all x1, waiting for transfers between devices, shards(): lax.all_to_all(result, ('sp', 'tp'), split_axis=0, concat_axis=0, tiled=T...  50.5 us
    dot_general x1, matrix products, expert_apply(): jnp.dot(hidden, down_w, preferred_element_type=jnp.float32)  9.96 us
    ppermute x3, starting transfers between devices, from_behind(): return lax.ppermute(value, axis, pairs)  9.84 us
    gather x1, local copies, waits for them, and re-layouts, shards(): returned.reshape(expert_count * capacity, model_width)[slot_of]  7.96 us
    reduce_sum x1, other arithmetic, shards(): routed = jnp.sum(weighted, axis=1)  6.41 us
    gather x1, local copies, waits for them, and re-layouts, shards(): padded_in[slot_source].reshape(expert_count, capacity, model_width)  6.02 us
    all_to_all x1, starting transfers between devices, shards(): lax.all_to_all(result, ('sp', 'tp'), split_axis=0, concat_axis=0, tiled=T...  5.67 us
  transfers between devices with their start and end apart: 4, of which 1 were waited for; matrix products, arithmetic and copies ran while one was open for 6% of the time, Pallas kernels for 0%

commit v1 on v0

v1 whole, which is shorter than its diff:
```python
import functools
import jax
import jax.numpy as jnp
from jax import lax
from jax.experimental import pallas as pl
from jax.experimental.pallas import tpu as pltpu
from jax.sharding import PartitionSpec as P

norm_eps = 1e-06
BF = jnp.bfloat16
F32 = jnp.float32
MIB = 1 << 20
LANES = 128

VM = pl.BlockSpec(memory_space=pltpu.VMEM)
SM = pl.BlockSpec(memory_space=pltpu.SMEM)
ANY = pl.BlockSpec(memory_space=pl.ANY)


def params(mib):
    return pltpu.CompilerParams(vmem_limit_bytes=mib * MIB)


def cost(flops, nbytes):
    return pl.CostEstimate(flops=flops, bytes_accessed=nbytes, transcendentals=0)


def dot(a, b):
    return jnp.dot(a, b, preferred_element_type=F32)


def slots_kernel(ids_ref, out_ref, *, capacity):
    slots, rows = out_ref.shape
    expert = lax.broadcasted_iota(jnp.int32, (slots, rows), 0) // capacity
    place = lax.broadcasted_iota(jnp.int32, (slots, rows), 0) % capacity
    named = expert == ids_ref[0:1, :]
    for k in range(1, ids_ref.shape[0]):
        named = jnp.logical_or(named, expert == ids_ref[k : k + 1, :])
    hit = named.astype(F32)
    before = lax.broadcasted_iota(jnp.int32, (rows, rows), 0) < lax.broadcasted_iota(
        jnp.int32, (rows, rows), 1
    )
    rank = dot(hit.astype(BF), before.astype(F32).astype(BF))
    out_ref[...] = jnp.where(rank == place.astype(F32), hit, 0.0).astype(BF)


def conv_kernel(
    half_ref, gate_ref, input_ref, value_ref, doc_ref, halo_ref, taps_ref, gain_ref,
    own_ref, send_ref, ext_ref, all_ref,
):
    rows, width = gate_ref.shape
    taps = taps_ref.shape[0]
    lead = taps - 1
    doc = jnp.transpose(jnp.broadcast_to(doc_ref[...].astype(F32), (LANES, rows)))
    ext_ref[8:, :width] = input_ref[...].astype(F32) * value_ref[...].astype(F32)
    ext_ref[8:, width:] = doc
    halo = halo_ref[...].astype(F32)
    ext_ref[8 - lead : 8, :width] = halo[0:lead] * halo[lead : 2 * lead]
    ext_ref[8 - lead : 8, width:] = halo[2 * lead : 3 * lead, :LANES]
    mixed = jnp.zeros((rows, width), F32)
    for tap in range(taps):
        start = 8 - lead + tap
        same = (ext_ref[start : start + rows, width:] == doc).astype(F32)
        same = jnp.concatenate([same] * (width // LANES), axis=1)
        mixed = mixed + taps_ref[tap : tap + 1, :].astype(F32) * ext_ref[start : start + rows, :width] * same
    branch = gate_ref[...].astype(F32) * mixed
    total = jnp.broadcast_to(jnp.sum(branch * branch, axis=1, keepdims=True), (rows, LANES))
    high = total.astype(BF).astype(F32)
    middle = (total - high).astype(BF).astype(F32)
    low = total - high - middle
    part = lax.broadcasted_iota(jnp.int32, (rows, LANES), 1) % 4
    packed = jnp.where(part == 0, high, jnp.where(part == 1, middle, jnp.where(part == 2, low, 0.0)))
    all_ref[:, :width] = branch * gain_ref[...].astype(F32)
    all_ref[:, width:] = packed
    half = half_ref[0]
    local = rows // 2
    own_ref[...] = all_ref[pl.ds(pl.multiple_of(half * local, local), local), :].astype(BF)
    send_ref[...] = all_ref[pl.ds(pl.multiple_of((1 - half) * local, local), local), :].astype(BF)


def mid_kernel(
    half_ref, own_ref, recv_ref, weight_ref, residual_ref, gain_ref, slots_ref,
    mid_ref, ffn_ref, out_ref, buf_ref, sems, *, chunks,
):
    width = weight_ref.shape[0] // 2
    half = half_ref[0]
    squares = jnp.sum(
        own_ref[:, width:].astype(F32) + recv_ref[:, width:].astype(F32), axis=1, keepdims=True
    ) * (4.0 / LANES)
    inv_rms = lax.rsqrt(squares / (2 * width) + norm_eps)
    update = dot(own_ref[:, :width], weight_ref[pl.ds(pl.multiple_of(half * width, width), width), :])
    update = update + dot(
        recv_ref[:, :width], weight_ref[pl.ds(pl.multiple_of((1 - half) * width, width), width), :]
    )
    mid = (residual_ref[...].astype(F32) + update * inv_rms).astype(BF)
    mid_ref[...] = mid
    mid_float = mid.astype(F32)
    mid_rms = lax.rsqrt(jnp.mean(mid_float * mid_float, axis=1, keepdims=True) + norm_eps)
    ffn = (mid_float * mid_rms * gain_ref[...].astype(F32)).astype(BF)
    ffn_ref[...] = ffn
    step = slots_ref.shape[0] // chunks
    copies = []
    for i in range(chunks):
        at = pl.ds(i * step, step)
        buf_ref[at, :] = dot(slots_ref[at, :], ffn).astype(BF)
        copies.append(pltpu.make_async_copy(buf_ref.at[at, :], out_ref.at[at, :], sems.at[i]))
        copies[-1].start()
    for copy in copies:
        copy.wait()


def expert_kernel(x_ref, gate_ref, up_ref, down_ref, out_ref, buf_ref, sems, *, chunks):
    step = x_ref.shape[0] // chunks
    copies = []
    for i in range(chunks):
        at = pl.ds(i * step, step)
        rows = x_ref[at, :]
        hidden = (jax.nn.silu(dot(rows, gate_ref[...])) * dot(rows, up_ref[...])).astype(BF)
        buf_ref[at, :] = dot(hidden, down_ref[...]).astype(BF)
        copies.append(pltpu.make_async_copy(buf_ref.at[at, :], out_ref.at[at, :], sems.at[i]))
        copies[-1].start()
    for copy in copies:
        copy.wait()


def shared_kernel(
    ffn_ref, mid_ref, gate_ref, up_ref, down_ref, ids_ref, share_ref, base_ref, mix_ref, *, capacity
):
    ffn = ffn_ref[...]
    hidden = (jax.nn.silu(dot(ffn, gate_ref[...])) * dot(ffn, up_ref[...])).astype(BF)
    base_ref[...] = mid_ref[...].astype(F32) + dot(hidden, down_ref[...])
    rows = ids_ref.shape[0]
    slots = mix_ref.shape[1]
    lane = lax.broadcasted_iota(jnp.int32, (rows, slots), 1)
    expert = lane // capacity
    place = (lane % capacity).astype(F32)
    hit = jnp.zeros((rows, slots), F32)
    share = jnp.zeros((rows, slots), F32)
    for k in range(ids_ref.shape[1]):
        named = expert == ids_ref[:, k : k + 1]
        hit = jnp.where(named, 1.0, hit)
        share = jnp.where(named, share_ref[:, k : k + 1], share)
    before = lax.broadcasted_iota(jnp.int32, (rows, rows), 1) < lax.broadcasted_iota(
        jnp.int32, (rows, rows), 0
    )
    rank = dot(before.astype(F32).astype(BF), hit.astype(BF))
    share = jnp.where(rank == place, share, 0.0)
    high = share.astype(BF)
    mix_ref[:rows, :] = high
    mix_ref[rows:, :] = (share - high.astype(F32)).astype(BF)


def combine_kernel(mix_ref, base_ref, back_ref, out_ref):
    rows = out_ref.shape[0]
    both = dot(mix_ref[...], back_ref[...])
    out_ref[...] = (base_ref[...] + (both[:rows] + both[rows:])).astype(BF)


def shards(
    residual, outer_gate, conv_input, conv_value, doc_ids, conv_taps, branch_gain, out_weight,
    ffn_gain, route_ids, route_weight, shared_gate, shared_up, shared_down,
    expert_gate, expert_up, expert_down,
):
    rows, width = conv_input.shape
    local, model = residual.shape
    top = route_ids.shape[1]
    lead = conv_taps.shape[0] - 1
    peers = lax.axis_size("sp")
    cores = lax.axis_size("tp")
    experts = peers * cores
    capacity = local * cores * top // experts
    slots = experts * capacity
    wide = width + LANES
    half = lax.axis_index("tp").astype(jnp.int32).reshape(1)

    doc_tail = jnp.broadcast_to(doc_ids[rows - lead :, None].astype(BF), (lead, width))
    tail = jnp.concatenate([conv_input[rows - lead :], conv_value[rows - lead :], doc_tail], axis=0)
    halo = lax.ppermute(tail, "sp", [(i, i + 1) for i in range(peers - 1)])

    slot_hot = pl.pallas_call(
        functools.partial(slots_kernel, capacity=capacity),
        out_shape=jax.ShapeDtypeStruct((slots, local), BF),
        in_specs=[VM], out_specs=VM, name="slots",
        compiler_params=params(8), cost_estimate=cost(2 * slots * local * local, slots * local * 2),
    )(route_ids.T)

    own, send = pl.pallas_call(
        conv_kernel,
        out_shape=[jax.ShapeDtypeStruct((local, wide), BF)] * 2,
        in_specs=[SM] + [VM] * 7, out_specs=[VM, VM], name="conv",
        scratch_shapes=[pltpu.VMEM((rows + 8, wide), F32), pltpu.VMEM((rows, wide), F32)],
        compiler_params=params(12),
    )(half, outer_gate, conv_input, conv_value, doc_ids.reshape(1, rows), halo, conv_taps, branch_gain.reshape(1, width))
    recv = lax.ppermute(send, "tp", [(0, 1), (1, 0)])

    chunks = 4
    mid, ffn, outgoing = pl.pallas_call(
        functools.partial(mid_kernel, chunks=chunks),
        out_shape=[jax.ShapeDtypeStruct((local, model), BF)] * 2 + [jax.ShapeDtypeStruct((slots, model), BF)],
        in_specs=[SM] + [VM] * 6, out_specs=[VM, VM, ANY], name="mid",
        scratch_shapes=[pltpu.VMEM((slots, model), BF), pltpu.SemaphoreType.DMA((chunks,))],
        compiler_params=params(24),
    )(half, own, recv, out_weight, residual, ffn_gain.reshape(1, model), slot_hot)

    arrived = lax.all_to_all(
        outgoing.reshape(experts, capacity, model), ("sp", "tp"), split_axis=0, concat_axis=0, tiled=True
    )
    result = pl.pallas_call(
        functools.partial(expert_kernel, chunks=chunks),
        out_shape=jax.ShapeDtypeStruct((slots, model), BF),
        in_specs=[VM] * 4, out_specs=ANY, name="expert",
        scratch_shapes=[pltpu.VMEM((slots, model), BF), pltpu.SemaphoreType.DMA((chunks,))],
        compiler_params=params(24),
    )(arrived.reshape(slots, model), expert_gate[0], expert_up[0], expert_down[0])
    result, ffn, mid = lax.optimization_barrier((result, ffn, mid))
    returned = lax.all_to_all(
        result.reshape(experts, capacity, model), ("sp", "tp"), split_axis=0, concat_axis=0, tiled=True
    ).reshape(slots, model)

    hidden = shared_gate.shape[1]
    base, mix = pl.pallas_call(
        functools.partial(shared_kernel, capacity=capacity),
        out_shape=[jax.ShapeDtypeStruct((local, model), F32), jax.ShapeDtypeStruct((2 * local, slots), BF)],
        in_specs=[VM] * 7, out_specs=[VM, VM], name="shared",
        compiler_params=params(24), cost_estimate=cost(40 * local * model * hidden, 6 * model * hidden),
    )(ffn, mid, shared_gate, shared_up, shared_down, route_ids, route_weight)

    block = model // 4
    return pl.pallas_call(
        combine_kernel,
        out_shape=jax.ShapeDtypeStruct((local, model), BF),
        grid=(model // block,), name="combine",
        in_specs=[
            pl.BlockSpec((2 * local, slots), lambda i: (0, 0)),
            pl.BlockSpec((local, block), lambda i: (0, i)),
            pl.BlockSpec((slots, block), lambda i: (0, i)),
        ],
        out_specs=pl.BlockSpec((local, block), lambda i: (0, i)),
        compiler_params=params(16),
    )(mix, base, returned)


def solution(mesh):
    placed = (
        P(("sp", "tp"), None), P("sp", "tp"), P("sp", "tp"), P("sp", "tp"), P("sp"), P(None, "tp"),
        P("tp"), P(), P(), P(("sp", "tp"), None), P(("sp", "tp"), None), P(), P(), P(),
        P(("sp", "tp"), None, None), P(("sp", "tp"), None, None), P(("sp", "tp"), None, None),
    )
    return jax.shard_map(
        shards, mesh=mesh, in_specs=placed, out_specs=P(("sp", "tp"), None), check_vma=False
    )
```

time: 200 us -> 159 us (0.80)
  matrix products: 23.1 us -> 0 us
  Pallas kernels: 0 us -> 17.9 us
  other arithmetic: 12.6 us -> 0.76 us
  local copies, waits for them, and re-layouts: 27.3 us -> 18.1 us
  blocking collectives: 69.9 us -> 63.6 us
  starting transfers between devices: 15.5 us -> 11.2 us
  waiting for transfers between devices: 50.5 us -> 46.4 us
    dot_general x5 -> x0, matrix products: 23.1 us -> none  [the longest x1 9.96 us: expert_apply(): jnp.dot(hidden, down_w, preferred_element_type=jnp.float32)]
    pallas_call x0 -> x6, Pallas kernels: none -> 17.9 us  [the longest x1 7.85 us: shards(): pl.pallas_call(functools.partial(expert_kernel, chunks=chunks), out_shape...]
    gather x2 -> x0, local copies, waits for them, and re-layouts: 14 us -> none  [the longest x1 7.96 us: shards(): returned.reshape(expert_count * capacity, model_width)[slot_of]]
    unnamed x21 -> x36, local copies, waits for them, and re-layouts: 3.87 us -> 15.1 us
    reduce_sum x4 -> x0, other arithmetic: 7.05 us -> none  [the longest x1 6.41 us: shards(): routed = jnp.sum(weighted, axis=1)]
    convert_element_type x1 -> x0, local copies, waits for them, and re-layouts: 4.75 us -> none  [shards(): returned_rows.astype(jnp.float32)]
    ppermute x3 -> x2, starting transfers between devices: 9.84 us -> 5.53 us  [the longest x1 3.92 us: shards(): halo = lax.ppermute(tail, 'sp', [(i, i + 1) for i in range(peers - 1)])]
    all_to_all x1, waiting for transfers between devices: 50.5 us -> 46.3 us  [shards(): lax.all_to_all(result.reshape(experts, capacity, model), ('sp', 'tp'), sp...]
  transfers between devices with their start and end apart: 4 -> 3, of which waited for: 1 -> 2; matrix products, arithmetic and copies ran while one was open for 6% -> 1% of each run, Pallas kernels for 0% -> 1%
where the time goes in v1:
time: 159 us; the launch traced here: 158 us
  blocking collectives  63.6 us (40%)
  waiting for transfers between devices  46.4 us (29%)
  local copies, waits for them, and re-layouts  18.1 us (11%)
  Pallas kernels  17.9 us (11%)
  starting transfers between devices  11.2 us (7%)
    all_to_all x1, blocking collectives, shards(): lax.all_to_all(outgoing.reshape(experts, capacity, model), ('sp', 'tp'),...  63.6 us
    all_to_all x1, waiting for transfers between devices, shards(): lax.all_to_all(result.reshape(experts, capacity, model), ('sp', 'tp'), sp...  46.3 us
    unnamed x36, local copies, waits for them, and re-layouts  15.1 us
    pallas_call x1, Pallas kernels, shards(): pl.pallas_call(functools.partial(expert_kernel, chunks=chunks), out_shape...  7.85 us
    all_to_all x1, starting transfers between devices, shards(): lax.all_to_all(result.reshape(experts, capacity, model), ('sp', 'tp'), sp...  5.64 us
    pallas_call x1, Pallas kernels, shards(): pl.pallas_call(combine_kernel, out_shape=jax.ShapeDtypeStruct((local, mod...  4.75 us
    ppermute x1, starting transfers between devices, shards(): halo = lax.ppermute(tail, 'sp', [(i, i + 1) for i in range(peers - 1)])  3.92 us
  transfers between devices with their start and end apart: 3, of which 2 were waited for; matrix products, arithmetic and copies ran while one was open for 1% of the time, Pallas kernels for 1%

profile of v1, /device:TPU:1, one launch (start us, length us, event | category | flops | bytes accessed | tf_op | source)
XLA Modules:
  0.0 158.1 jit_solution(4621345256666926030)
XLA Ops:
  0.0 0.7 convert.3
  0.8 0.7 slice.10
  1.5 0.7 slice.11
  2.3 3.9 %collective-permute-start = (bf16[6,512]{1,0:T(8,128)(2,1)S(1)}, bf16[6,512]{1,0:T(8,128)(2,1)S(1)}, u32[]{:S(2)}, u32[]{:S(2)}) collective-permute-start(bf16[6,512]{1,0:T(8,128)(2,1)S(1)} %maximum_maximum_fusion), channel_id=1, source_target_pairs={{0,2},{2,4},{4,6},{6,8},{8,10},{10,12},{12,14},{14,16},{16,18},{18... | collective-permute-start | bytes 18440 | tf_op jit(solution)/shard_map/ppermute | solution.py:178
  6.2 0.7 reshape.28.gain_ref
  7.0 0.9 copy-done.6
  8.0 0.9 copy-done.7
  8.9 0.9 copy-done.8
  9.9 0.7 copy-done.11
  11.9 1.6 %collective-permute-start.1 = (bf16[128,640]{1,0:T(8,128)(2,1)S(1)}, bf16[128,640]{1,0:T(8,128)(2,1)S(1)}, u32[]{:S(2)}, u32[]{:S(2)}) collective-permute-start(bf16[128,640]{1,0:T(8,128)(2,1)S(1)} %get-tuple-element.16), channel_id=1, source_target_pairs={{0,1},{1,0},{2,3},{3,2},{4,5},{5,4},{6,7},{7,6},{8,9},{9,8},{10,11... | collective-permute-start | bytes 491528 | tf_op jit(solution)/shard_map/ppermute | solution.py:194
  13.5 0.7 reshape.29.gain_ref
  15.3 2.2 %copy-done.1 = bf16[1024,2048]{1,0:T(8,128)(2,1)S(1)} copy-done((bf16[1024,2048]{1,0:T(8,128)(2,1)S(1)}, bf16[1024,2048]{1,0:T(8,128)(2,1)}, u32[]{:S(2)}) %copy-start.1) | copy-done | bytes 4194328
  17.4 1.0 copy-done.5
  18.5 2.9 %mid.1 = (bf16[128,2048]{1,0:T(8,128)(2,1)S(1)}, bf16[128,2048]{1,0:T(8,128)(2,1)S(1)}, bf16[1024,2048]{1,0:T(8,128)(2,1)S(1)}) custom-call(s32[1]{0:T(128)} %bitcast.half_ref, bf16[128,640]{1,0:T(8,128)(2,1)S(1)} %get-tuple-element.15.own_ref, bf16[128,640]{1,0:T(8,128)(2,1)S(1)} %collective-permute-done.1.recv_ref, bf16[1024,2048]{1,0:T(8,128)(2,1)S(1)} %copy-done.1, ...), custom_call_target="tpu_custom_call" | custom-call | tf_op jit(solution)/shard_map/mid/pallas_call | solution.py:197
  21.4 63.6 %all_to_all.10 = bf16[128,8,2048]{2,1,0:T(8,128)(2,1)S(1)} all-to-all(bf16[128,8,2048]{2,1,0:T(8,128)(2,1)S(1)} %bitcast.12), channel_id=1, replica_groups=mesh['sp'=64,'tp'=2] {'sp','tp'}, dimensions={0} | all-to-all | bytes 8388608 | tf_op jit(solution)/shard_map/all_to_all | solution.py:205
  85.1 7.8 %expert.1 = bf16[1024,2048]{1,0:T(8,128)(2,1)S(1)} custom-call(bf16[1024,2048]{1,0:T(8,128)(2,1)S(1)} %bitcast.11, bf16[2048,512]{1,0:T(8,128)(2,1)S(1)} %bitcast.13, bf16[2048,512]{1,0:T(8,128)(2,1)S(1)} %bitcast.14, bf16[512,2048]{1,0:T(8,128)(2,1)S(1)} %bitcast.15), custom_call_target="tpu_custom_call" | custom-call | tf_op jit(solution)/shard_map/expert/pallas_call | solution.py:208
  93.0 2.0 %copy-done = bf16[1024,2048]{1,0:T(8,128)(2,1)} copy-done((bf16[1024,2048]{1,0:T(8,128)(2,1)}, bf16[1024,2048]{1,0:T(8,128)(2,1)S(1)}, u32[]{:S(2)}) %copy-start) | copy-done | bytes 4194328
  95.0 5.6 %all-to-all-start.1 = ((bf16[128,8,2048]{2,1,0:T(8,128)(2,1)}), bf16[128,8,2048]{2,1,0:T(8,128)(2,1)}, u32[]{:S(2)}, u32[]{:S(2)}) async-start(bf16[128,8,2048]{2,1,0:T(8,128)(2,1)} %bitcast.10), calls=%async_computation.1 | async-start | bytes 8388608 | tf_op jit(solution)/shard_map/all_to_all | solution.py:216
  100.9 1.6 %copy-done.13 = bf16[2048,512]{1,0:T(8,128)(2,1)S(1)} copy-done((bf16[2048,512]{1,0:T(8,128)(2,1)S(1)}, bf16[2048,512]{1,0:T(8,128)(2,1)}, u32[]{:S(2)}) %copy-start.13) | copy-done | bytes 2097176
  102.4 1.6 %copy-done.14 = bf16[2048,512]{1,0:T(8,128)(2,1)S(1)} copy-done((bf16[2048,512]{1,0:T(8,128)(2,1)S(1)}, bf16[2048,512]{1,0:T(8,128)(2,1)}, u32[]{:S(2)}) %copy-start.14) | copy-done | bytes 2097176
  104.0 1.6 %copy-done.15 = bf16[512,2048]{1,0:T(8,128)(2,1)S(1)} copy-done((bf16[512,2048]{1,0:T(8,128)(2,1)S(1)}, bf16[512,2048]{1,0:T(8,128)(2,1)}, u32[]{:S(2)}) %copy-start.15) | copy-done | bytes 2097176
  105.6 1.4 shared.1
  107.0 46.3 %all-to-all-done.1 = bf16[128,8,2048]{2,1,0:T(8,128)(2,1)} async-done(((bf16[128,8,2048]{2,1,0:T(8,128)(2,1)}), bf16[128,8,2048]{2,1,0:T(8,128)(2,1)}, u32[]{:S(2)}, u32[]{:S(2)}) %all-to-all-start.1) | async-done | bytes 4194336 | tf_op jit(solution)/shard_map/all_to_all | solution.py:216
  153.3 4.7 %combine.1 = bf16[128,2048]{1,0:T(8,128)(2,1)} custom-call(bf16[256,1024]{1,0:T(8,128)(2,1)S(1)} %get-tuple-element.22.mix_ref, f32[128,2048]{1,0:T(8,128)S(1)} %get-tuple-element.23.base_ref, bf16[1024,2048]{1,0:T(8,128)(2,1)} %bitcast.9.back_ref), custom_call_target="tpu_custom_call" | custom-call | tf_op jit(solution)/shard_map/combine/pallas_call | solution.py:229
  (33 shorter events, 3.0 us)
Async XLA Ops:
  2.3 4.7 %collective-permute-start = (bf16[6,512]{1,0:T(8,128)(2,1)S(1)}, bf16[6,512]{1,0:T(8,128)(2,1)S(1)}, u32[]{:S(2)}, u32[]{:S(2)}) collective-permute-start(bf16[6,512]{1,0:T(8,128)(2,1)S(1)} %maximum_maximum_fusion), channel_id=1, source_target_pairs={{0,2},{2,4},{4,6},{6,8},{8,10},{10,12},{12,14},{14,16},{16,18},{18... | collective-permute-start | bytes 18440 | tf_op jit(solution)/shard_map/ppermute | solution.py:178
  7.0 0.9 copy-start.6
  8.0 0.9 copy-start.7
  8.9 0.9 copy-start.8
  9.9 0.7 copy-start.11
  10.6 0.7 copy-start.12
  11.9 3.4 %collective-permute-start.1 = (bf16[128,640]{1,0:T(8,128)(2,1)S(1)}, bf16[128,640]{1,0:T(8,128)(2,1)S(1)}, u32[]{:S(2)}, u32[]{:S(2)}) collective-permute-start(bf16[128,640]{1,0:T(8,128)(2,1)S(1)} %get-tuple-element.16), channel_id=1, source_target_pairs={{0,1},{1,0},{2,3},{3,2},{4,5},{5,4},{6,7},{7,6},{8,9},{9,8},{10,11... | collective-permute-start | bytes 491528 | tf_op jit(solution)/shard_map/ppermute | solution.py:194
  14.2 0.7 copy-start.9
  15.2 2.2 %copy-start.1 = (bf16[1024,2048]{1,0:T(8,128)(2,1)S(1)}, bf16[1024,2048]{1,0:T(8,128)(2,1)}, u32[]{:S(2)}) copy-start(bf16[1024,2048]{1,0:T(8,128)(2,1)} %weight_ref.1) | copy-start | bytes 12582916
  17.4 1.0 copy-start.5
  21.4 63.7 %copy-start.2 = (bf16[1,2048,512]{2,1,0:T(8,128)(2,1)S(1)}, bf16[1,2048,512]{2,1,0:T(8,128)(2,1)}, u32[]{:S(2)}) copy-start(bf16[1,2048,512]{2,1,0:T(8,128)(2,1)} %param.31) | copy-start | bytes 6291460
  21.4 63.7 %copy-start.3 = (bf16[1,2048,512]{2,1,0:T(8,128)(2,1)S(1)}, bf16[1,2048,512]{2,1,0:T(8,128)(2,1)}, u32[]{:S(2)}) copy-start(bf16[1,2048,512]{2,1,0:T(8,128)(2,1)} %param.32) | copy-start | bytes 6291460
  21.4 63.7 %copy-start.4 = (bf16[1,512,2048]{2,1,0:T(8,128)(2,1)S(1)}, bf16[1,512,2048]{2,1,0:T(8,128)(2,1)}, u32[]{:S(2)}) copy-start(bf16[1,512,2048]{2,1,0:T(8,128)(2,1)} %param.33) | copy-start | bytes 6291460
  93.0 2.0 %copy-start = (bf16[1024,2048]{1,0:T(8,128)(2,1)}, bf16[1024,2048]{1,0:T(8,128)(2,1)S(1)}, u32[]{:S(2)}) copy-start(bf16[1024,2048]{1,0:T(8,128)(2,1)S(1)} %expert.1) | copy-start | bytes 12582916
  95.0 5.7 %copy-start.10 = (s32[128,4]{0,1:T(4,128)S(1)}, s32[128,4]{0,1:T(4,128)}, u32[]{:S(2)}) copy-start(s32[128,4]{0,1:T(4,128)} %param.26) | copy-start | bytes 6148
  95.0 5.8 %copy-start.16 = (f32[128,4]{0,1:T(4,128)S(1)}, f32[128,4]{0,1:T(4,128)}, u32[]{:S(2)}) copy-start(f32[128,4]{0,1:T(4,128)} %param.27) | copy-start | bytes 6148
  95.0 58.4 %all-to-all-start.1 = ((bf16[128,8,2048]{2,1,0:T(8,128)(2,1)}), bf16[128,8,2048]{2,1,0:T(8,128)(2,1)}, u32[]{:S(2)}, u32[]{:S(2)}) async-start(bf16[128,8,2048]{2,1,0:T(8,128)(2,1)} %bitcast.10), calls=%async_computation.1 | async-start | bytes 8388608 | tf_op jit(solution)/shard_map/all_to_all | solution.py:216
  100.8 1.6 %copy-start.13 = (bf16[2048,512]{1,0:T(8,128)(2,1)S(1)}, bf16[2048,512]{1,0:T(8,128)(2,1)}, u32[]{:S(2)}) copy-start(bf16[2048,512]{1,0:T(8,128)(2,1)} %gate_ref.3) | copy-start | bytes 6291460
  102.4 1.6 %copy-start.14 = (bf16[2048,512]{1,0:T(8,128)(2,1)S(1)}, bf16[2048,512]{1,0:T(8,128)(2,1)}, u32[]{:S(2)}) copy-start(bf16[2048,512]{1,0:T(8,128)(2,1)} %up_ref.1) | copy-start | bytes 6291460
  104.0 1.6 %copy-start.15 = (bf16[512,2048]{1,0:T(8,128)(2,1)S(1)}, bf16[512,2048]{1,0:T(8,128)(2,1)}, u32[]{:S(2)}) copy-start(bf16[512,2048]{1,0:T(8,128)(2,1)} %down_ref.1) | copy-start | bytes 6291460

commit v2 on v1

v2 whole, which is shorter than its diff:
```python
import functools
import jax
import jax.numpy as jnp
from jax import lax
from jax.experimental import pallas as pl
from jax.experimental.pallas import tpu as pltpu
from jax.sharding import PartitionSpec as P

norm_eps = 1e-06
BF = jnp.bfloat16
F32 = jnp.float32
MIB = 1 << 20
LANES = 128

VM = pl.BlockSpec(memory_space=pltpu.VMEM)
SM = pl.BlockSpec(memory_space=pltpu.SMEM)
HBM = pl.BlockSpec(memory_space=pltpu.HBM)
LONG = 1 << 33


def params(mib):
    return pltpu.CompilerParams(vmem_limit_bytes=mib * MIB)


def cost(flops, nbytes):
    return pl.CostEstimate(flops=flops, bytes_accessed=nbytes, transcendentals=0)


def dot(a, b):
    return jnp.dot(a, b, preferred_element_type=F32)


def tail_kernel(input_ref, value_ref, doc_ref, tail_ref):
    width = input_ref.shape[1]
    tail_ref[0:8, :] = input_ref[8:16, :]
    tail_ref[8:16, :] = value_ref[8:16, :]
    last = jnp.transpose(jnp.broadcast_to(doc_ref[...].astype(F32), (LANES, LANES)))
    tail_ref[16:24, :] = jnp.concatenate([last[LANES - 8 :, :].astype(BF)] * (width // LANES), axis=1)


def slots_kernel(ids_ref, share_ref, hot_ref, mix_ref, *, capacity):
    slots, rows = hot_ref.shape
    slot = lax.broadcasted_iota(jnp.int32, (slots, rows), 0)
    expert = slot // capacity
    place = (slot % capacity).astype(F32)
    hit = jnp.zeros((slots, rows), F32)
    share = jnp.zeros((slots, rows), F32)
    for k in range(ids_ref.shape[0]):
        named = expert == ids_ref[k : k + 1, :]
        hit = jnp.where(named, 1.0, hit)
        share = jnp.where(named, share_ref[k : k + 1, :], share)
    before = lax.broadcasted_iota(jnp.int32, (rows, rows), 0) < lax.broadcasted_iota(
        jnp.int32, (rows, rows), 1
    )
    mine = dot(hit.astype(BF), before.astype(F32).astype(BF)) == place
    hot_ref[...] = jnp.where(mine, hit, 0.0).astype(BF)
    share = jnp.transpose(jnp.where(mine, share, 0.0))
    high = share.astype(BF)
    mix_ref[:rows, :] = high
    mix_ref[rows:, :] = (share - high.astype(F32)).astype(BF)


def conv_kernel(
    half_ref, gate_ref, input_ref, value_ref, doc_ref, halo_ref, taps_ref, gain_ref,
    own_ref, send_ref, ext_ref, all_ref,
):
    rows, width = gate_ref.shape
    taps = taps_ref.shape[0]
    doc = jnp.transpose(jnp.broadcast_to(doc_ref[...].astype(F32), (LANES, rows)))
    ext_ref[8:, :width] = input_ref[...].astype(F32) * value_ref[...].astype(F32)
    ext_ref[8:, width:] = doc
    ext_ref[0:8, :width] = halo_ref[0:8, :].astype(F32) * halo_ref[8:16, :].astype(F32)
    ext_ref[0:8, width:] = halo_ref[16:24, :LANES].astype(F32)
    mixed = jnp.zeros((rows, width), F32)
    for tap in range(taps):
        start = 9 - taps + tap
        same = (ext_ref[start : start + rows, width:] == doc).astype(F32)
        same = jnp.concatenate([same] * (width // LANES), axis=1)
        mixed = mixed + taps_ref[tap : tap + 1, :].astype(F32) * ext_ref[start : start + rows, :width] * same
    branch = gate_ref[...].astype(F32) * mixed
    total = jnp.broadcast_to(jnp.sum(branch * branch, axis=1, keepdims=True), (rows, LANES))
    high = total.astype(BF).astype(F32)
    middle = (total - high).astype(BF).astype(F32)
    low = total - high - middle
    part = lax.broadcasted_iota(jnp.int32, (rows, LANES), 1) % 4
    packed = jnp.where(part == 0, high, jnp.where(part == 1, middle, jnp.where(part == 2, low, 0.0)))
    all_ref[:, :width] = branch * gain_ref[...].astype(F32)
    all_ref[:, width:] = packed
    half = half_ref[0]
    local = rows // 2
    own_ref[...] = all_ref[pl.ds(pl.multiple_of(half * local, local), local), :].astype(BF)
    send_ref[...] = all_ref[pl.ds(pl.multiple_of((1 - half) * local, local), local), :].astype(BF)


def mid_kernel(
    half_ref, own_ref, recv_ref, weight_ref, residual_ref, gain_ref, slots_ref,
    mid_ref, ffn_ref, out_ref, *, chunks,
):
    width = weight_ref.shape[0] // 2
    half = half_ref[0]
    squares = jnp.sum(
        own_ref[:, width:].astype(F32) + recv_ref[:, width:].astype(F32), axis=1, keepdims=True
    ) * (4.0 / LANES)
    inv_rms = lax.rsqrt(squares / (2 * width) + norm_eps)
    update = dot(own_ref[:, :width], weight_ref[pl.ds(pl.multiple_of(half * width, width), width), :])
    update = update + dot(
        recv_ref[:, :width], weight_ref[pl.ds(pl.multiple_of((1 - half) * width, width), width), :]
    )
    mid = (residual_ref[...].astype(F32) + update * inv_rms).astype(BF)
    mid_ref[...] = mid
    mid_float = mid.astype(F32)
    mid_rms = lax.rsqrt(jnp.mean(mid_float * mid_float, axis=1, keepdims=True) + norm_eps)
    ffn = (mid_float * mid_rms * gain_ref[...].astype(F32)).astype(BF)
    ffn_ref[...] = ffn
    step = slots_ref.shape[0] // chunks
    for i in range(chunks):
        at = pl.ds(i * step, step)
        out_ref[at, :] = dot(slots_ref[at, :], ffn).astype(BF)


def expert_kernel(
    x_ref, gate_ref, up_ref, down_ref, ffn_ref, mid_ref, shared_gate_ref, shared_up_ref, shared_down_ref,
    out_ref, base_ref, *, chunks,
):
    def apply(rows, gate, up, down):
        hidden = (jax.nn.silu(dot(rows, gate[...])) * dot(rows, up[...])).astype(BF)
        return dot(hidden, down[...])

    shared = apply(ffn_ref[...], shared_gate_ref, shared_up_ref, shared_down_ref)
    base_ref[...] = mid_ref[...].astype(F32) + shared
    step = x_ref.shape[0] // chunks
    for i in range(chunks):
        at = pl.ds(i * step, step)
        out_ref[at, :] = apply(x_ref[at, :], gate_ref, up_ref, down_ref).astype(BF)


def combine_kernel(mix_ref, base_ref, back_ref, out_ref):
    rows = out_ref.shape[0]
    both = dot(mix_ref[...], back_ref[...])
    out_ref[...] = (base_ref[...] + (both[:rows] + both[rows:])).astype(BF)


def shards(
    residual, outer_gate, conv_input, conv_value, doc_ids, conv_taps, branch_gain, out_weight,
    ffn_gain, route_ids, route_weight, shared_gate, shared_up, shared_down,
    expert_gate, expert_up, expert_down,
):
    rows, width = conv_input.shape
    local, model = residual.shape
    top = route_ids.shape[1]
    peers = lax.axis_size("sp")
    cores = lax.axis_size("tp")
    experts = peers * cores
    capacity = local * cores * top // experts
    slots = experts * capacity
    wide = width + LANES
    half = lax.axis_index("tp").astype(jnp.int32).reshape(1)

    doc = doc_ids.reshape(1, rows)
    tail = pl.pallas_call(
        tail_kernel,
        out_shape=jax.ShapeDtypeStruct((24, width), BF),
        grid=(1,), name="tail",
        in_specs=[
            pl.BlockSpec((16, width), lambda i: (rows // 16 - 1, 0)),
            pl.BlockSpec((16, width), lambda i: (rows // 16 - 1, 0)),
            pl.BlockSpec((1, LANES), lambda i: (0, rows // LANES - 1)),
        ],
        out_specs=pl.BlockSpec((24, width), lambda i: (0, 0)),
        compiler_params=params(4), cost_estimate=cost(LONG, 0),
    )(*[pltpu.with_memory_space_constraint(a, pltpu.HBM) for a in (conv_input, conv_value, doc)])
    halo = lax.ppermute(tail, "sp", [(i, i + 1) for i in range(peers - 1)])

    own, send = pl.pallas_call(
        conv_kernel,
        out_shape=[jax.ShapeDtypeStruct((local, wide), BF)] * 2,
        in_specs=[SM] + [VM] * 7, out_specs=[VM, VM], name="conv",
        scratch_shapes=[pltpu.VMEM((rows + 8, wide), F32), pltpu.VMEM((rows, wide), F32)],
        compiler_params=params(6), cost_estimate=cost(LONG, 0),
    )(half, outer_gate, conv_input, conv_value, doc, halo, conv_taps, branch_gain.reshape(1, width))
    recv = lax.ppermute(send, "tp", [(0, 1), (1, 0)])

    slot_hot, mix = pl.pallas_call(
        functools.partial(slots_kernel, capacity=capacity),
        out_shape=[jax.ShapeDtypeStruct((slots, local), BF), jax.ShapeDtypeStruct((2 * local, slots), BF)],
        in_specs=[VM] * 2, out_specs=[VM] * 2, name="slots",
        compiler_params=params(6), cost_estimate=cost(LONG, 0),
    )(route_ids.T, route_weight.T)

    chunks = 4
    mid, ffn, outgoing = pl.pallas_call(
        functools.partial(mid_kernel, chunks=chunks),
        out_shape=[jax.ShapeDtypeStruct((local, model), BF)] * 2 + [jax.ShapeDtypeStruct((slots, model), BF)],
        in_specs=[SM] + [VM] * 6, out_specs=[VM, VM, VM], name="mid",
        compiler_params=params(12), cost_estimate=cost(LONG, 0),
    )(half, own, recv, out_weight, residual, ffn_gain.reshape(1, model), slot_hot)

    arrived = lax.all_to_all(
        outgoing.reshape(experts, capacity, model), ("sp", "tp"), split_axis=0, concat_axis=0, tiled=True
    ).reshape(slots, model)
    result, base = pl.pallas_call(
        functools.partial(expert_kernel, chunks=chunks),
        out_shape=[jax.ShapeDtypeStruct((slots, model), BF), jax.ShapeDtypeStruct((local, model), F32)],
        in_specs=[VM] * 9, out_specs=[VM] * 2, name="expert",
        compiler_params=params(12), cost_estimate=cost(LONG, 0),
    )(arrived, expert_gate[0], expert_up[0], expert_down[0], ffn, mid, shared_gate, shared_up, shared_down)
    returned = lax.all_to_all(
        result.reshape(experts, capacity, model), ("sp", "tp"), split_axis=0, concat_axis=0, tiled=True
    ).reshape(slots, model)

    return pl.pallas_call(
        combine_kernel,
        out_shape=jax.ShapeDtypeStruct((local, model), BF),
        in_specs=[VM] * 3, out_specs=VM, name="combine",
        compiler_params=params(8), cost_estimate=cost(LONG, 0),
    )(mix, base, returned)


def solution(mesh):
    placed = (
        P(("sp", "tp"), None), P("sp", "tp"), P("sp", "tp"), P("sp", "tp"), P("sp"), P(None, "tp"),
        P("tp"), P(), P(), P(("sp", "tp"), None), P(("sp", "tp"), None), P(), P(), P(),
        P(("sp", "tp"), None, None), P(("sp", "tp"), None, None), P(("sp", "tp"), None, None),
    )
    return jax.shard_map(
        shards, mesh=mesh, in_specs=placed, out_specs=P(("sp", "tp"), None), check_vma=False
    )
```

time: 159 us -> 143 us (0.90)
  blocking collectives: 63.6 us -> 121 us
  waiting for transfers between devices: 46.4 us -> 1.23 us
  local copies, waits for them, and re-layouts: 18.1 us -> 1.5 us
  starting transfers between devices: 11.2 us -> 5.55 us
  Pallas kernels: 17.9 us -> 14.2 us
    all_to_all x0 -> x1, blocking collectives: none -> 56.8 us  [shards(): lax.all_to_all(result.reshape(experts, capacity, model), ('sp', 'tp'), sp...]
    all_to_all x1 -> x0, waiting for transfers between devices: 46.3 us -> none  [shards(): lax.all_to_all(result.reshape(experts, capacity, model), ('sp', 'tp'), sp...]
    unnamed x36 -> x34, local copies, waits for them, and re-layouts: 15.1 us -> 1.49 us
    all_to_all x1 -> x0, starting transfers between devices: 5.64 us -> none  [shards(): lax.all_to_all(result.reshape(experts, capacity, model), ('sp', 'tp'), sp...]
    pallas_call x1, Pallas kernels: 4.75 us -> 2.07 us  [shards(): pl.pallas_call(combine_kernel, out_shape=jax.ShapeDtypeStruct((local, mod...]
  transfers between devices with their start and end apart: 3 -> 2, of which waited for: 2 -> 2; matrix products, arithmetic and copies ran while one was open for 1% -> 0% of each run, Pallas kernels for 1% -> 0%
where the time goes in v2:
time: 143 us
  blocking collectives  121 us (85%)
  Pallas kernels  14.2 us (10%)
  starting transfers between devices  5.55 us (4%)
  local copies, waits for them, and re-layouts  1.5 us (1%)
    all_to_all x1, blocking collectives, shards(): lax.all_to_all(outgoing.reshape(experts, capacity, model), ('sp', 'tp'),...  63.7 us
    all_to_all x1, blocking collectives, shards(): lax.all_to_all(result.reshape(experts, capacity, model), ('sp', 'tp'), sp...  56.8 us
    pallas_call x1, Pallas kernels, shards(): pl.pallas_call(functools.partial(expert_kernel, chunks=chunks), out_shape...  7.94 us
    ppermute x1, starting transfers between devices, shards(): halo = lax.ppermute(tail, 'sp', [(i, i + 1) for i in range(peers - 1)])  3.94 us
  transfers between devices with their start and end apart: 2, of which 2 were waited for; matrix products, arithmetic and copies ran while one was open for 0% of the time, Pallas kernels for 0%

profile of v2, /device:TPU:1, one launch (start us, length us, event | category | flops | bytes accessed | tf_op | source)
XLA Modules:
  0.0 143.2 jit_solution(17858425526737686396)
XLA Ops:
  0.0 0.9 tail.1
  0.9 3.9 %collective-permute-start = (bf16[24,512]{1,0:T(8,128)(2,1)S(1)}, bf16[24,512]{1,0:T(8,128)(2,1)S(1)}, u32[]{:S(2)}, u32[]{:S(2)}) collective-permute-start(bf16[24,512]{1,0:T(8,128)(2,1)S(1)} %tail.1), channel_id=1, source_target_pairs={{0,2},{2,4},{4,6},{6,8},{8,10},{10,12},{12,14},{14,16},{16,18},{18... | collective-permute-start | bytes 73736 | tf_op jit(solution)/shard_map/ppermute | solution.py:172
  4.9 0.0 copy-done.16
  4.9 0.9 collective-permute-done.halo_ref
  5.8 0.0 copy-done.9
  5.8 0.0 copy-start.12
  5.8 0.0 copy-start.13
  5.9 0.6 conv.1
  6.5 1.6 %collective-permute-start.1 = (bf16[128,640]{1,0:T(8,128)(2,1)S(1)}, bf16[128,640]{1,0:T(8,128)(2,1)S(1)}, u32[]{:S(2)}, u32[]{:S(2)}) collective-permute-start(bf16[128,640]{1,0:T(8,128)(2,1)S(1)} %get-tuple-element.16), channel_id=1, source_target_pairs={{0,1},{1,0},{2,3},{3,2},{4,5},{5,4},{6,7},{7,6},{8,9},{9,8},{10,11... | collective-permute-start | bytes 491528 | tf_op jit(solution)/shard_map/ppermute | solution.py:181
  8.1 0.0 copy-start.7
  8.1 0.5 slots.1
  8.7 0.1 copy-done.15
  8.8 0.3 collective-permute-done.1.recv_ref
  9.1 1.2 copy-done
  10.3 0.1 copy-done.7
  10.4 2.2 %mid.1 = (bf16[128,2048]{1,0:T(8,128)(2,1)S(1)}, bf16[128,2048]{1,0:T(8,128)(2,1)S(1)}, bf16[1024,2048]{1,0:T(8,128)(2,1)S(1)}) custom-call(s32[1]{0:T(128)} %bitcast.2.half_ref, bf16[128,640]{1,0:T(8,128)(2,1)S(1)} %get-tuple-element.15.own_ref, bf16[128,640]{1,0:T(8,128)(2,1)S(1)} %collective-permute-done.1.recv_ref, bf16[1024,2048]{1,0:T(8,128)(2,1)S(1)} %copy-done, ...), custom_call_target="tpu_custom_call" | custom-call | flops 8589934592 | tf_op jit(solution)/shard_map/mid/pallas_call | solution.py:191
  12.6 0.0 copy-start.1
  12.6 0.0 copy-start.2
  12.6 0.0 copy-start.3
  12.6 0.0 copy-start.4
  12.6 63.7 %all_to_all.10 = bf16[128,8,2048]{2,1,0:T(8,128)(2,1)S(1)} all-to-all(bf16[128,8,2048]{2,1,0:T(8,128)(2,1)S(1)} %bitcast.11), channel_id=1, replica_groups=mesh['sp'=64,'tp'=2] {'sp','tp'}, dimensions={0} | all-to-all | bytes 8388608 | tf_op jit(solution)/shard_map/all_to_all | solution.py:198
  76.3 7.9 %expert.1 = (bf16[1024,2048]{1,0:T(8,128)(2,1)S(1)}, f32[128,2048]{1,0:T(8,128)S(1)}) custom-call(bf16[1024,2048]{1,0:T(8,128)(2,1)S(1)} %bitcast.12, bf16[2048,512]{1,0:T(8,128)(2,1)S(1)} %bitcast.15, bf16[2048,512]{1,0:T(8,128)(2,1)S(1)} %bitcast.16, bf16[512,2048]{1,0:T(8,128)(2,1)S(1)} %bitcast.17, bf16[128,2048]{1,0:T(8,128)(2,1)S(1)} %get-tuple-element.19.ffn_ref, ...), custom_call_target="tpu_custom_call" | custom-call | flops 8589934592 | tf_op jit(solution)/shard_map/expert/pallas_call | solution.py:201
  84.3 56.8 %all_to_all.11 = bf16[128,8,2048]{2,1,0:T(8,128)(2,1)S(1)} all-to-all(bf16[128,8,2048]{2,1,0:T(8,128)(2,1)S(1)} %bitcast.13), channel_id=1, replica_groups=mesh['sp'=64,'tp'=2] {'sp','tp'}, dimensions={0} | all-to-all | bytes 8388608 | tf_op jit(solution)/shard_map/all_to_all | solution.py:207
  141.1 2.1 %combine.1 = bf16[128,2048]{1,0:T(8,128)(2,1)} custom-call(bf16[256,1024]{1,0:T(8,128)(2,1)S(1)} %get-tuple-element.14.mix_ref, f32[128,2048]{1,0:T(8,128)S(1)} %get-tuple-element.21.base_ref, bf16[1024,2048]{1,0:T(8,128)(2,1)S(1)} %bitcast.14), custom_call_target="tpu_custom_call" | custom-call | flops 8589934592 | tf_op jit(solution)/shard_map/combine/pallas_call | solution.py:211
  (24 shorter events, 0.1 us)
Async XLA Ops:
  0.0 4.9 %copy-start.16 = (bf16[512]{0:T(512)(128)(2,1)S(1)}, bf16[512]{0:T(512)(128)(2,1)}, u32[]{:S(2)}) copy-start(bf16[512]{0:T(512)(128)(2,1)} %param.23) | copy-start | bytes 3076
  0.0 5.8 %copy-start.8 = (bf16[256,512]{1,0:T(8,128)(2,1)S(1)}, bf16[256,512]{1,0:T(8,128)(2,1)}, u32[]{:S(2)}) copy-start(bf16[256,512]{1,0:T(8,128)(2,1)} %gate_ref.1) | copy-start | bytes 786436
  0.0 5.8 %copy-start.9 = (bf16[256,512]{1,0:T(8,128)(2,1)S(1)}, bf16[256,512]{1,0:T(8,128)(2,1)}, u32[]{:S(2)}) copy-start(bf16[256,512]{1,0:T(8,128)(2,1)} %input_ref.3) | copy-start | bytes 786436
  0.0 5.8 %copy-start.10 = (bf16[256,512]{1,0:T(8,128)(2,1)S(1)}, bf16[256,512]{1,0:T(8,128)(2,1)}, u32[]{:S(2)}) copy-start(bf16[256,512]{1,0:T(8,128)(2,1)} %value_ref.3) | copy-start | bytes 786436
  0.0 5.8 %copy-start.11 = (bf16[3,512]{1,0:T(4,128)(2,1)S(1)}, bf16[3,512]{1,0:T(4,128)(2,1)}, u32[]{:S(2)}) copy-start(bf16[3,512]{1,0:T(4,128)(2,1)} %taps_ref.1) | copy-start | bytes 9220
  0.0 5.8 %copy-start.14 = (s32[256]{0:T(256)S(1)}, s32[256]{0:T(256)}, u32[]{:S(2)}) copy-start(s32[256]{0:T(256)} %param.21) | copy-start | bytes 3076
  0.9 4.9 %collective-permute-start = (bf16[24,512]{1,0:T(8,128)(2,1)S(1)}, bf16[24,512]{1,0:T(8,128)(2,1)S(1)}, u32[]{:S(2)}, u32[]{:S(2)}) collective-permute-start(bf16[24,512]{1,0:T(8,128)(2,1)S(1)} %tail.1), channel_id=1, source_target_pairs={{0,2},{2,4},{4,6},{6,8},{8,10},{10,12},{12,14},{14,16},{16,18},{18... | collective-permute-start | bytes 73736 | tf_op jit(solution)/shard_map/ppermute | solution.py:172
  5.8 2.3 %copy-start.12 = (s32[128,4]{0,1:T(4,128)S(1)}, s32[128,4]{0,1:T(4,128)}, u32[]{:S(2)}) copy-start(s32[128,4]{0,1:T(4,128)} %param.26) | copy-start | bytes 6148
  5.8 2.3 %copy-start.13 = (f32[128,4]{0,1:T(4,128)S(1)}, f32[128,4]{0,1:T(4,128)}, u32[]{:S(2)}) copy-start(f32[128,4]{0,1:T(4,128)} %param.27) | copy-start | bytes 6148
  6.5 2.6 %collective-permute-start.1 = (bf16[128,640]{1,0:T(8,128)(2,1)S(1)}, bf16[128,640]{1,0:T(8,128)(2,1)S(1)}, u32[]{:S(2)}, u32[]{:S(2)}) collective-permute-start(bf16[128,640]{1,0:T(8,128)(2,1)S(1)} %get-tuple-element.16), channel_id=1, source_target_pairs={{0,1},{1,0},{2,3},{3,2},{4,5},{5,4},{6,7},{7,6},{8,9},{9,8},{10,11... | collective-permute-start | bytes 491528 | tf_op jit(solution)/shard_map/ppermute | solution.py:181
  8.1 0.7 copy-start.15
  8.1 2.2 %copy-start = (bf16[1024,2048]{1,0:T(8,128)(2,1)S(1)}, bf16[1024,2048]{1,0:T(8,128)(2,1)}, u32[]{:S(2)}) copy-start(bf16[1024,2048]{1,0:T(8,128)(2,1)} %weight_ref.1) | copy-start | bytes 12582916
  8.1 2.3 %copy-start.7 = (bf16[128,2048]{1,0:T(8,128)(2,1)S(1)}, bf16[128,2048]{1,0:T(8,128)(2,1)}, u32[]{:S(2)}) copy-start(bf16[128,2048]{1,0:T(8,128)(2,1)} %residual_ref.1) | copy-start | bytes 1572868
  10.4 65.9 %copy-start.5 = (bf16[2048,512]{1,0:T(8,128)(2,1)S(1)}, bf16[2048,512]{1,0:T(8,128)(2,1)}, u32[]{:S(2)}) copy-start(bf16[2048,512]{1,0:T(8,128)(2,1)} %shared_up_ref.1) | copy-start | bytes 6291460
  10.4 65.9 %copy-start.6 = (bf16[512,2048]{1,0:T(8,128)(2,1)S(1)}, bf16[512,2048]{1,0:T(8,128)(2,1)}, u32[]{:S(2)}) copy-start(bf16[512,2048]{1,0:T(8,128)(2,1)} %shared_down_ref.1) | copy-start | bytes 6291460
  12.6 63.7 %copy-start.1 = (bf16[1,2048,512]{2,1,0:T(8,128)(2,1)S(1)}, bf16[1,2048,512]{2,1,0:T(8,128)(2,1)}, u32[]{:S(2)}) copy-start(bf16[1,2048,512]{2,1,0:T(8,128)(2,1)} %param.31) | copy-start | bytes 6291460
  12.6 63.7 %copy-start.2 = (bf16[1,2048,512]{2,1,0:T(8,128)(2,1)S(1)}, bf16[1,2048,512]{2,1,0:T(8,128)(2,1)}, u32[]{:S(2)}) copy-start(bf16[1,2048,512]{2,1,0:T(8,128)(2,1)} %param.32) | copy-start | bytes 6291460
  12.6 63.7 %copy-start.3 = (bf16[1,512,2048]{2,1,0:T(8,128)(2,1)S(1)}, bf16[1,512,2048]{2,1,0:T(8,128)(2,1)}, u32[]{:S(2)}) copy-start(bf16[1,512,2048]{2,1,0:T(8,128)(2,1)} %param.33) | copy-start | bytes 6291460
  12.6 63.7 %copy-start.4 = (bf16[2048,512]{1,0:T(8,128)(2,1)S(1)}, bf16[2048,512]{1,0:T(8,128)(2,1)}, u32[]{:S(2)}) copy-start(bf16[2048,512]{1,0:T(8,128)(2,1)} %shared_gate_ref.1) | copy-start | bytes 6291460

commit v3 on v2

--- a/solution.py
+++ b/solution.py
@@ -16,6 +16,7 @@
 SM = pl.BlockSpec(memory_space=pltpu.SMEM)
 HBM = pl.BlockSpec(memory_space=pltpu.HBM)
 LONG = 1 << 33
+SHORT = 1 << 31
 
 
 def params(mib):
@@ -134,10 +135,20 @@
         out_ref[at, :] = apply(x_ref[at, :], gate_ref, up_ref, down_ref).astype(BF)
 
 
-def combine_kernel(mix_ref, base_ref, back_ref, out_ref):
-    rows = out_ref.shape[0]
-    both = dot(mix_ref[...], back_ref[...])
-    out_ref[...] = (base_ref[...] + (both[:rows] + both[rows:])).astype(BF)
+def combine_kernel(mix_ref, base_ref, back_ref, out_ref, buf_ref, sems):
+    rows, width = buf_ref.shape
+    chunks = sems.shape[0]
+    step = width // chunks
+    mix = mix_ref[...]
+    copies = []
+    for i in range(chunks):
+        at = pl.ds(i * step, step)
+        both = dot(mix, back_ref[:, at])
+        buf_ref[:, at] = (base_ref[:, at] + (both[:rows] + both[rows:])).astype(BF)
+        copies.append(pltpu.make_async_copy(buf_ref.at[:, at], out_ref.at[:, at], sems.at[i]))
+        copies[-1].start()
+    for copy in copies:
+        copy.wait()
 
 
 def shards(
@@ -171,21 +182,22 @@
     )(*[pltpu.with_memory_space_constraint(a, pltpu.HBM) for a in (conv_input, conv_value, doc)])
     halo = lax.ppermute(tail, "sp", [(i, i + 1) for i in range(peers - 1)])
 
+    slot_hot, mix = pl.pallas_call(
+        functools.partial(slots_kernel, capacity=capacity),
+        out_shape=[jax.ShapeDtypeStruct((slots, local), BF), jax.ShapeDtypeStruct((2 * local, slots), BF)],
+        in_specs=[VM] * 2, out_specs=[VM] * 2, name="slots",
+        compiler_params=params(6), cost_estimate=cost(SHORT, 0),
+    )(route_ids.T, route_weight.T)
+
+    halo, slot_hot, mix = lax.optimization_barrier((halo, slot_hot, mix))
     own, send = pl.pallas_call(
         conv_kernel,
         out_shape=[jax.ShapeDtypeStruct((local, wide), BF)] * 2,
         in_specs=[SM] + [VM] * 7, out_specs=[VM, VM], name="conv",
         scratch_shapes=[pltpu.VMEM((rows + 8, wide), F32), pltpu.VMEM((rows, wide), F32)],
-        compiler_params=params(6), cost_estimate=cost(LONG, 0),
+        compiler_params=params(6), cost_estimate=cost(SHORT, 0),
     )(half, outer_gate, conv_input, conv_value, doc, halo, conv_taps, branch_gain.reshape(1, width))
     recv = lax.ppermute(send, "tp", [(0, 1), (1, 0)])
-
-    slot_hot, mix = pl.pallas_call(
-        functools.partial(slots_kernel, capacity=capacity),
-        out_shape=[jax.ShapeDtypeStruct((slots, local), BF), jax.ShapeDtypeStruct((2 * local, slots), BF)],
-        in_specs=[VM] * 2, out_specs=[VM] * 2, name="slots",
-        compiler_params=params(6), cost_estimate=cost(LONG, 0),
-    )(route_ids.T, route_weight.T)
 
     chunks = 4
     mid, ffn, outgoing = pl.pallas_call(
@@ -211,7 +223,8 @@
     return pl.pallas_call(
         combine_kernel,
         out_shape=jax.ShapeDtypeStruct((local, model), BF),
-        in_specs=[VM] * 3, out_specs=VM, name="combine",
+        in_specs=[VM] * 3, out_specs=HBM, name="combine",
+        scratch_shapes=[pltpu.VMEM((local, model), BF), pltpu.SemaphoreType.DMA((4,))],
         compiler_params=params(8), cost_estimate=cost(LONG, 0),
     )(mix, base, returned)
 

time: 143 us -> 142 us (level)
  no operation moved by 1% of the time
where the time goes in v3:
time: 142 us
  blocking collectives  121 us (85%)
  Pallas kernels  14.1 us (10%)
  starting transfers between devices  5.36 us (4%)
    all_to_all x1, blocking collectives, shards(): lax.all_to_all(outgoing.reshape(experts, capacity, model), ('sp', 'tp'),...  64.1 us
    all_to_all x1, blocking collectives, shards(): lax.all_to_all(result.reshape(experts, capacity, model), ('sp', 'tp'), sp...  56.9 us
    pallas_call x1, Pallas kernels, shards(): pl.pallas_call(functools.partial(expert_kernel, chunks=chunks), out_shape...  7.95 us
    ppermute x1, starting transfers between devices, shards(): halo = lax.ppermute(tail, 'sp', [(i, i + 1) for i in range(peers - 1)])  3.94 us
  transfers between devices with their start and end apart: 2, of which 2 were waited for; matrix products, arithmetic and copies ran while one was open for 0% of the time, Pallas kernels for 0%

profile of v3, /device:TPU:1, one launch (start us, length us, event | category | flops | bytes accessed | tf_op | source)
XLA Modules:
  0.0 142.2 jit_solution(11513635004122817192)
XLA Ops:
  0.0 0.8 tail.1
  0.9 3.9 %collective-permute-start = (bf16[24,512]{1,0:T(8,128)(2,1)S(1)}, bf16[24,512]{1,0:T(8,128)(2,1)S(1)}, u32[]{:S(2)}, u32[]{:S(2)}) collective-permute-start(bf16[24,512]{1,0:T(8,128)(2,1)S(1)} %tail.1), channel_id=1, source_target_pairs={{0,2},{2,4},{4,6},{6,8},{8,10},{10,12},{12,14},{14,16},{16,18},{18... | collective-permute-start | bytes 73736 | tf_op jit(solution)/shard_map/ppermute | solution.py:183
  4.8 0.0 copy-start.16
  4.8 0.0 copy-start.8
  4.8 0.0 copy-start.9
  4.9 0.0 copy-start.10
  4.9 0.0 copy-start.11
  4.9 0.0 copy-start.14
  4.9 0.5 slots.1
  5.4 0.1 copy-done.16
  5.5 0.2 collective-permute-done.halo_ref
  5.7 0.1 copy-done.8
  5.8 0.1 copy-done.9
  5.9 0.1 copy-done.10
  6.0 0.6 conv.1
  6.6 1.4 collective-permute-start.1
  8.0 1.0 collective-permute-done.1.recv_ref
  9.1 2.2 %mid.1 = (bf16[128,2048]{1,0:T(8,128)(2,1)S(1)}, bf16[128,2048]{1,0:T(8,128)(2,1)S(1)}, bf16[1024,2048]{1,0:T(8,128)(2,1)S(1)}) custom-call(s32[1]{0:T(128)} %bitcast.3.half_ref, bf16[128,640]{1,0:T(8,128)(2,1)S(1)} %get-tuple-element.21.own_ref, bf16[128,640]{1,0:T(8,128)(2,1)S(1)} %collective-permute-done.1.recv_ref, bf16[1024,2048]{1,0:T(8,128)(2,1)S(1)} %copy-done, ...), custom_call_target="tpu_custom_call" | custom-call | flops 8589934592 | tf_op jit(solution)/shard_map/mid/pallas_call | solution.py:203
  11.3 0.0 copy-start.1
  11.3 0.0 copy-start.2
  11.3 64.1 %all_to_all.10 = bf16[128,8,2048]{2,1,0:T(8,128)(2,1)S(1)} all-to-all(bf16[128,8,2048]{2,1,0:T(8,128)(2,1)S(1)} %bitcast.11), channel_id=1, replica_groups=mesh['sp'=64,'tp'=2] {'sp','tp'}, dimensions={0} | all-to-all | bytes 8388608 | tf_op jit(solution)/shard_map/all_to_all | solution.py:210
  75.4 7.9 %expert.1 = (bf16[1024,2048]{1,0:T(8,128)(2,1)S(1)}, f32[128,2048]{1,0:T(8,128)S(1)}) custom-call(bf16[1024,2048]{1,0:T(8,128)(2,1)S(1)} %bitcast.12, bf16[2048,512]{1,0:T(8,128)(2,1)S(1)} %bitcast.15, bf16[2048,512]{1,0:T(8,128)(2,1)S(1)} %bitcast.16, bf16[512,2048]{1,0:T(8,128)(2,1)S(1)} %bitcast.17, bf16[128,2048]{1,0:T(8,128)(2,1)S(1)} %get-tuple-element.25.ffn_ref, ...), custom_call_target="tpu_custom_call" | custom-call | flops 8589934592 | tf_op jit(solution)/shard_map/expert/pallas_call | solution.py:213
  83.4 56.9 %all_to_all.11 = bf16[128,8,2048]{2,1,0:T(8,128)(2,1)S(1)} all-to-all(bf16[128,8,2048]{2,1,0:T(8,128)(2,1)S(1)} %bitcast.13), channel_id=1, replica_groups=mesh['sp'=64,'tp'=2] {'sp','tp'}, dimensions={0} | all-to-all | bytes 8388608 | tf_op jit(solution)/shard_map/all_to_all | solution.py:219
  140.2 1.9 %combine.1 = bf16[128,2048]{1,0:T(8,128)(2,1)} custom-call(bf16[256,1024]{1,0:T(8,128)(2,1)S(1)} %get-tuple-element.19.mix_ref, f32[128,2048]{1,0:T(8,128)S(1)} %get-tuple-element.27.base_ref, bf16[1024,2048]{1,0:T(8,128)(2,1)S(1)} %bitcast.14), custom_call_target="tpu_custom_call" | custom-call | flops 8589934592 | tf_op jit(solution)/shard_map/combine/pallas_call | solution.py:223
  (24 shorter events, 0.1 us)
Async XLA Ops:
  0.0 4.8 %copy-start.12 = (s32[128,4]{0,1:T(4,128)S(1)}, s32[128,4]{0,1:T(4,128)}, u32[]{:S(2)}) copy-start(s32[128,4]{0,1:T(4,128)} %param.26) | copy-start | bytes 6148
  0.0 4.8 %copy-start.13 = (f32[128,4]{0,1:T(4,128)S(1)}, f32[128,4]{0,1:T(4,128)}, u32[]{:S(2)}) copy-start(f32[128,4]{0,1:T(4,128)} %param.27) | copy-start | bytes 6148
  0.9 4.9 %collective-permute-start = (bf16[24,512]{1,0:T(8,128)(2,1)S(1)}, bf16[24,512]{1,0:T(8,128)(2,1)S(1)}, u32[]{:S(2)}, u32[]{:S(2)}) collective-permute-start(bf16[24,512]{1,0:T(8,128)(2,1)S(1)} %tail.1), channel_id=1, source_target_pairs={{0,2},{2,4},{4,6},{6,8},{8,10},{10,12},{12,14},{14,16},{16,18},{18... | collective-permute-start | bytes 73736 | tf_op jit(solution)/shard_map/ppermute | solution.py:183
  4.8 0.7 copy-start.16
  4.8 1.0 copy-start.8
  4.8 1.0 copy-start.9
  4.9 1.1 copy-start.10
  4.9 1.1 copy-start.11
  4.9 1.1 copy-start.14
  6.0 2.1 %copy-start.15 = (bf16[2048]{0:T(1024)(128)(2,1)S(1)}, bf16[2048]{0:T(1024)(128)(2,1)}, u32[]{:S(2)}) copy-start(bf16[2048]{0:T(1024)(128)(2,1)} %param.25) | copy-start | bytes 12292
  6.0 3.1 %copy-start = (bf16[1024,2048]{1,0:T(8,128)(2,1)S(1)}, bf16[1024,2048]{1,0:T(8,128)(2,1)}, u32[]{:S(2)}) copy-start(bf16[1024,2048]{1,0:T(8,128)(2,1)} %weight_ref.1) | copy-start | bytes 12582916
  6.0 3.1 %copy-start.7 = (bf16[128,2048]{1,0:T(8,128)(2,1)S(1)}, bf16[128,2048]{1,0:T(8,128)(2,1)}, u32[]{:S(2)}) copy-start(bf16[128,2048]{1,0:T(8,128)(2,1)} %residual_ref.1) | copy-start | bytes 1572868
  6.6 2.4 %collective-permute-start.1 = (bf16[128,640]{1,0:T(8,128)(2,1)S(1)}, bf16[128,640]{1,0:T(8,128)(2,1)S(1)}, u32[]{:S(2)}, u32[]{:S(2)}) collective-permute-start(bf16[128,640]{1,0:T(8,128)(2,1)S(1)} %get-tuple-element.22), channel_id=1, source_target_pairs={{0,1},{1,0},{2,3},{3,2},{4,5},{5,4},{6,7},{7,6},{8,9},{9,8},{10,11... | collective-permute-start | bytes 491528 | tf_op jit(solution)/shard_map/ppermute | solution.py:200
  9.1 66.3 %copy-start.5 = (bf16[2048,512]{1,0:T(8,128)(2,1)S(1)}, bf16[2048,512]{1,0:T(8,128)(2,1)}, u32[]{:S(2)}) copy-start(bf16[2048,512]{1,0:T(8,128)(2,1)} %shared_up_ref.1) | copy-start | bytes 6291460
  9.1 66.3 %copy-start.6 = (bf16[512,2048]{1,0:T(8,128)(2,1)S(1)}, bf16[512,2048]{1,0:T(8,128)(2,1)}, u32[]{:S(2)}) copy-start(bf16[512,2048]{1,0:T(8,128)(2,1)} %shared_down_ref.1) | copy-start | bytes 6291460
  11.3 64.1 %copy-start.1 = (bf16[1,2048,512]{2,1,0:T(8,128)(2,1)S(1)}, bf16[1,2048,512]{2,1,0:T(8,128)(2,1)}, u32[]{:S(2)}) copy-start(bf16[1,2048,512]{2,1,0:T(8,128)(2,1)} %param.31) | copy-start | bytes 6291460
  11.3 64.1 %copy-start.2 = (bf16[1,2048,512]{2,1,0:T(8,128)(2,1)S(1)}, bf16[1,2048,512]{2,1,0:T(8,128)(2,1)}, u32[]{:S(2)}) copy-start(bf16[1,2048,512]{2,1,0:T(8,128)(2,1)} %param.32) | copy-start | bytes 6291460
  11.3 64.1 %copy-start.3 = (bf16[1,512,2048]{2,1,0:T(8,128)(2,1)S(1)}, bf16[1,512,2048]{2,1,0:T(8,128)(2,1)}, u32[]{:S(2)}) copy-start(bf16[1,512,2048]{2,1,0:T(8,128)(2,1)} %param.33) | copy-start | bytes 6291460
  11.3 64.1 %copy-start.4 = (bf16[2048,512]{1,0:T(8,128)(2,1)S(1)}, bf16[2048,512]{1,0:T(8,128)(2,1)}, u32[]{:S(2)}) copy-start(bf16[2048,512]{1,0:T(8,128)(2,1)} %shared_gate_ref.1) | copy-start | bytes 6291460

commit v4 on v3

--- a/solution.py
+++ b/solution.py
@@ -17,6 +17,7 @@
 HBM = pl.BlockSpec(memory_space=pltpu.HBM)
 LONG = 1 << 33
 SHORT = 1 << 31
+LEAD = 1 << 31
 
 
 def params(mib):
@@ -39,7 +40,7 @@
     tail_ref[16:24, :] = jnp.concatenate([last[LANES - 8 :, :].astype(BF)] * (width // LANES), axis=1)
 
 
-def slots_kernel(ids_ref, share_ref, hot_ref, mix_ref, *, capacity):
+def fill_slots(ids_ref, share_ref, hot_ref, mix_ref, capacity):
     slots, rows = hot_ref.shape
     slot = lax.broadcasted_iota(jnp.int32, (slots, rows), 0)
     expert = slot // capacity
@@ -61,52 +62,90 @@
     mix_ref[rows:, :] = (share - high.astype(F32)).astype(BF)
 
 
-def conv_kernel(
-    half_ref, gate_ref, input_ref, value_ref, doc_ref, halo_ref, taps_ref, gain_ref,
-    own_ref, send_ref, ext_ref, all_ref,
-):
-    rows, width = gate_ref.shape
+def convolve(gate, ext_ref, taps_ref, gain_ref):
+    rows, width = gate.shape
     taps = taps_ref.shape[0]
-    doc = jnp.transpose(jnp.broadcast_to(doc_ref[...].astype(F32), (LANES, rows)))
-    ext_ref[8:, :width] = input_ref[...].astype(F32) * value_ref[...].astype(F32)
-    ext_ref[8:, width:] = doc
-    ext_ref[0:8, :width] = halo_ref[0:8, :].astype(F32) * halo_ref[8:16, :].astype(F32)
-    ext_ref[0:8, width:] = halo_ref[16:24, :LANES].astype(F32)
+    doc = ext_ref[8 : 8 + rows, width:]
     mixed = jnp.zeros((rows, width), F32)
     for tap in range(taps):
         start = 9 - taps + tap
         same = (ext_ref[start : start + rows, width:] == doc).astype(F32)
         same = jnp.concatenate([same] * (width // LANES), axis=1)
         mixed = mixed + taps_ref[tap : tap + 1, :].astype(F32) * ext_ref[start : start + rows, :width] * same
-    branch = gate_ref[...].astype(F32) * mixed
+    branch = gate.astype(F32) * mixed
     total = jnp.broadcast_to(jnp.sum(branch * branch, axis=1, keepdims=True), (rows, LANES))
     high = total.astype(BF).astype(F32)
     middle = (total - high).astype(BF).astype(F32)
     low = total - high - middle
     part = lax.broadcasted_iota(jnp.int32, (rows, LANES), 1) % 4
     packed = jnp.where(part == 0, high, jnp.where(part == 1, middle, jnp.where(part == 2, low, 0.0)))
-    all_ref[:, :width] = branch * gain_ref[...].astype(F32)
-    all_ref[:, width:] = packed
+    return (branch * gain_ref[...].astype(F32)).astype(BF), packed.astype(BF)
+
+
+def early_kernel(
+    half_ref, gate_ref, input_ref, value_ref, doc_ref, taps_ref, gain_ref, ids_ref, share_ref, weight_ref,
+    own_ref, send_ref, hot_ref, mix_ref, near_ref, far_ref, ext_ref, all_ref, sems, *, capacity,
+):
     half = half_ref[0]
+    size = near_ref.shape[0]
+    copies = [
+        pltpu.make_async_copy(weight_ref.at[pl.ds(pl.multiple_of(which * size, size), size), :], to, sems.at[i])
+        for i, (which, to) in enumerate(((half, near_ref), (1 - half, far_ref)))
+    ]
+    for copy in copies:
+        copy.start()
+    rows, width = gate_ref.shape
+    ext_ref[0:8, :] = jnp.zeros((8, width + LANES), F32)
+    ext_ref[8:, :width] = input_ref[...].astype(F32) * value_ref[...].astype(F32)
+    ext_ref[8:, width:] = jnp.transpose(jnp.broadcast_to(doc_ref[...].astype(F32), (LANES, rows)))
+    all_ref[:, :width], all_ref[:, width:] = convolve(gate_ref[...], ext_ref, taps_ref, gain_ref)
     local = rows // 2
-    own_ref[...] = all_ref[pl.ds(pl.multiple_of(half * local, local), local), :].astype(BF)
-    send_ref[...] = all_ref[pl.ds(pl.multiple_of((1 - half) * local, local), local), :].astype(BF)
+    own_ref[...] = all_ref[pl.ds(pl.multiple_of(half * local, local), local), :]
+    send_ref[...] = all_ref[pl.ds(pl.multiple_of((1 - half) * local, local), local), :]
+    fill_slots(ids_ref, share_ref, hot_ref, mix_ref, capacity)
+    for copy in copies:
+        copy.wait()
+
+
+def lead_kernel(
+    half_ref, own_in_ref, send_in_ref, gate_ref, input_ref, value_ref, doc_ref, halo_ref, taps_ref, gain_ref,
+    own_ref, send_ref, ext_ref,
+):
+    width = gate_ref.shape[1]
+    ext_ref[0:8, :width] = halo_ref[0:8, :].astype(F32) * halo_ref[8:16, :].astype(F32)
+    ext_ref[0:8, width:] = halo_ref[16:24, :LANES].astype(F32)
+    ext_ref[8:24, :width] = input_ref[0:16, :].astype(F32) * value_ref[0:16, :].astype(F32)
+    doc = jnp.transpose(jnp.broadcast_to(doc_ref[:, :LANES].astype(F32), (LANES, LANES)))
+    ext_ref[8:24, width:] = doc[0:16, :]
+    scaled, packed = convolve(gate_ref[0:16, :], ext_ref, taps_ref, gain_ref)
+    own_ref[...] = own_in_ref[...]
+    send_ref[...] = send_in_ref[...]
+
+    @pl.when(half_ref[0] == 0)
+    def _():
+        own_ref[0:16, :width] = scaled
+        own_ref[0:16, width:] = packed
+
+    @pl.when(half_ref[0] == 1)
+    def _():
+        send_ref[0:16, :width] = scaled
+        send_ref[0:16, width:] = packed
+
+
+def half_kernel(own_ref, near_ref, part_ref):
+    part_ref[...] = dot(own_ref[:, : near_ref.shape[0]], near_ref[...])
 
 
 def mid_kernel(
-    half_ref, own_ref, recv_ref, weight_ref, residual_ref, gain_ref, slots_ref,
+    own_ref, recv_ref, part_ref, far_ref, residual_ref, gain_ref, slots_ref,
     mid_ref, ffn_ref, out_ref, *, chunks,
 ):
-    width = weight_ref.shape[0] // 2
-    half = half_ref[0]
+    width = far_ref.shape[0]
     squares = jnp.sum(
         own_ref[:, width:].astype(F32) + recv_ref[:, width:].astype(F32), axis=1, keepdims=True
     ) * (4.0 / LANES)
     inv_rms = lax.rsqrt(squares / (2 * width) + norm_eps)
-    update = dot(own_ref[:, :width], weight_ref[pl.ds(pl.multiple_of(half * width, width), width), :])
-    update = update + dot(
-        recv_ref[:, :width], weight_ref[pl.ds(pl.multiple_of((1 - half) * width, width), width), :]
-    )
+    update = part_ref[...] + dot(recv_ref[:, :width], far_ref[...])
     mid = (residual_ref[...].astype(F32) + update * inv_rms).astype(BF)
     mid_ref[...] = mid
     mid_float = mid.astype(F32)
@@ -182,30 +221,47 @@
     )(*[pltpu.with_memory_space_constraint(a, pltpu.HBM) for a in (conv_input, conv_value, doc)])
     halo = lax.ppermute(tail, "sp", [(i, i + 1) for i in range(peers - 1)])
 
-    slot_hot, mix = pl.pallas_call(
-        functools.partial(slots_kernel, capacity=capacity),
-        out_shape=[jax.ShapeDtypeStruct((slots, local), BF), jax.ShapeDtypeStruct((2 * local, slots), BF)],
-        in_specs=[VM] * 2, out_specs=[VM] * 2, name="slots",
-        compiler_params=params(6), cost_estimate=cost(SHORT, 0),
-    )(route_ids.T, route_weight.T)
-
-    halo, slot_hot, mix = lax.optimization_barrier((halo, slot_hot, mix))
+    gain = branch_gain.reshape(1, width)
+    mover = jax.ShapeDtypeStruct((local, wide), BF)
+    piece = jax.ShapeDtypeStruct((width, model), BF)
+    own, send, slot_hot, mix, near, far = pl.pallas_call(
+        functools.partial(early_kernel, capacity=capacity),
+        out_shape=[
+            mover, mover, jax.ShapeDtypeStruct((slots, local), BF), jax.ShapeDtypeStruct((2 * local, slots), BF),
+            piece, piece,
+        ],
+        in_specs=[SM] + [VM] * 8 + [HBM], out_specs=[VM] * 6, name="early",
+        scratch_shapes=[
+            pltpu.VMEM((rows + 8, wide), F32), pltpu.VMEM((rows, wide), BF), pltpu.SemaphoreType.DMA((2,)),
+        ],
+        compiler_params=params(12), cost_estimate=cost(SHORT, 0),
+    )(
+        half, outer_gate, conv_input, conv_value, doc, conv_taps, gain, route_ids.T, route_weight.T,
+        pltpu.with_memory_space_constraint(out_weight, pltpu.HBM),
+    )
+    halo, own, send = lax.optimization_barrier((halo, own, send))
     own, send = pl.pallas_call(
-        conv_kernel,
-        out_shape=[jax.ShapeDtypeStruct((local, wide), BF)] * 2,
-        in_specs=[SM] + [VM] * 7, out_specs=[VM, VM], name="conv",
-        scratch_shapes=[pltpu.VMEM((rows + 8, wide), F32), pltpu.VMEM((rows, wide), F32)],
-        compiler_params=params(6), cost_estimate=cost(SHORT, 0),
-    )(half, outer_gate, conv_input, conv_value, doc, halo, conv_taps, branch_gain.reshape(1, width))
+        lead_kernel,
+        out_shape=[mover, mover],
+        in_specs=[SM] + [VM] * 9, out_specs=[VM, VM], name="lead",
+        scratch_shapes=[pltpu.VMEM((24, wide), F32)],
+        compiler_params=params(6), cost_estimate=cost(LEAD, 0),
+    )(half, own, send, outer_gate, conv_input, conv_value, doc, halo, conv_taps, gain)
     recv = lax.ppermute(send, "tp", [(0, 1), (1, 0)])
+    part = pl.pallas_call(
+        half_kernel,
+        out_shape=jax.ShapeDtypeStruct((local, model), F32),
+        in_specs=[VM, VM], out_specs=VM, name="half",
+        compiler_params=params(6), cost_estimate=cost(LEAD, 0),
+    )(own, near)
 
     chunks = 4
     mid, ffn, outgoing = pl.pallas_call(
         functools.partial(mid_kernel, chunks=chunks),
         out_shape=[jax.ShapeDtypeStruct((local, model), BF)] * 2 + [jax.ShapeDtypeStruct((slots, model), BF)],
-        in_specs=[SM] + [VM] * 6, out_specs=[VM, VM, VM], name="mid",
+        in_specs=[VM] * 7, out_specs=[VM, VM, VM], name="mid",
         compiler_params=params(12), cost_estimate=cost(LONG, 0),
-    )(half, own, recv, out_weight, residual, ffn_gain.reshape(1, model), slot_hot)
+    )(own, recv, part, far, residual, ffn_gain.reshape(1, model), slot_hot)
 
     arrived = lax.all_to_all(
         outgoing.reshape(experts, capacity, model), ("sp", "tp"), split_axis=0, concat_axis=0, tiled=True

time: 142 us -> 142 us (level)
  Pallas kernels: 14.1 us -> 16.6 us
    pallas_call x2 -> x3, Pallas kernels: 1.17 us -> 3.89 us  [the longest x1 3.25 us: shards(): pl.pallas_call(functools.partial(early_kernel, capacity=capacity), out_sh...]
  transfers between devices with their start and end apart: 2 -> 2, of which waited for: 2 -> 1; matrix products, arithmetic and copies ran while one was open for 0% -> 0% of each run, Pallas kernels for 0% -> 3%
where the time goes in v4:
time: 142 us
  blocking collectives  120 us (85%)
  Pallas kernels  16.6 us (12%)
  starting transfers between devices  4.94 us (3%)
    all_to_all x1, blocking collectives, shards(): lax.all_to_all(outgoing.reshape(experts, capacity, model), ('sp', 'tp'),...  62.8 us
    all_to_all x1, blocking collectives, shards(): lax.all_to_all(result.reshape(experts, capacity, model), ('sp', 'tp'), sp...  56.9 us
    pallas_call x1, Pallas kernels, shards(): pl.pallas_call(functools.partial(expert_kernel, chunks=chunks), out_shape...  7.93 us
    ppermute x1, starting transfers between devices, shards(): halo = lax.ppermute(tail, 'sp', [(i, i + 1) for i in range(peers - 1)])  3.94 us
    pallas_call x1, Pallas kernels, shards(): pl.pallas_call(functools.partial(early_kernel, capacity=capacity), out_sh...  3.25 us
  transfers between devices with their start and end apart: 2, of which 1 were waited for; matrix products, arithmetic and copies ran while one was open for 0% of the time, Pallas kernels for 3%

profile of v4, /device:TPU:1, one launch (start us, length us, event | category | flops | bytes accessed | tf_op | source)
XLA Modules:
  0.0 142.1 jit_solution(14602621950864854586)
XLA Ops:
  0.0 0.0 copy-start.9
  0.0 0.0 copy-start.10
  0.0 0.0 copy-start.11
  0.0 0.0 copy-start.12
  0.1 0.9 tail.1
  0.9 3.9 %collective-permute-start = (bf16[24,512]{1,0:T(8,128)(2,1)S(1)}, bf16[24,512]{1,0:T(8,128)(2,1)S(1)}, u32[]{:S(2)}, u32[]{:S(2)}) collective-permute-start(bf16[24,512]{1,0:T(8,128)(2,1)S(1)} %tail.1), channel_id=1, source_target_pairs={{0,2},{2,4},{4,6},{6,8},{8,10},{10,12},{12,14},{14,16},{16,18},{18... | collective-permute-start | bytes 73736 | tf_op jit(solution)/shard_map/ppermute | solution.py:222
  5.0 0.0 copy-start.14
  5.0 3.3 %early.1 = (bf16[128,640]{1,0:T(8,128)(2,1)S(1)}, bf16[128,640]{1,0:T(8,128)(2,1)S(1)}, bf16[1024,128]{1,0:T(8,128)(2,1)S(1)}, bf16[256,1024]{1,0:T(8,128)(2,1)S...) custom-call(s32[1]{0:T(128)} %bitcast.half_ref, bf16[256,512]{1,0:T(8,128)(2,1)S(1)} %copy-done.7, ...), custom_call_target="tpu_custom_call" | custom-call | flops 2147483648 | tf_op jit(solution)/shard_map/early/pallas_call | solution.py:227
  8.3 0.0 collective-permute-done.halo_ref
  8.3 0.2 lead.1
  8.5 1.0 collective-permute-start.1
  9.5 0.5 half.1.part_ref
  9.9 0.6 collective-permute-done.1.recv_ref
  10.5 0.0 copy-done.6
  10.5 1.9 %mid.1 = (bf16[128,2048]{1,0:T(8,128)(2,1)S(1)}, bf16[128,2048]{1,0:T(8,128)(2,1)S(1)}, bf16[1024,2048]{1,0:T(8,128)(2,1)S(1)}) custom-call(bf16[128,640]{1,0:T(8,128)(2,1)S(1)} %get-tuple-element.27.own_ref, bf16[128,640]{1,0:T(8,128)(2,1)S(1)} %collective-permute-done.1.recv_ref, f32[128,2048]{1,0:T(8,128)S(1)} %half.1.part_ref, ...), custom_call_target="tpu_custom_call" | custom-call | flops 8589934592 | tf_op jit(solution)/shard_map/mid/pallas_call | solution.py:259
  12.4 0.0 copy-start
  12.4 0.0 copy-start.1
  12.5 0.0 copy-start.2
  12.5 0.0 copy-start.3
  12.5 62.8 %all_to_all.10 = bf16[128,8,2048]{2,1,0:T(8,128)(2,1)S(1)} all-to-all(bf16[128,8,2048]{2,1,0:T(8,128)(2,1)S(1)} %bitcast.11), channel_id=1, replica_groups=mesh['sp'=64,'tp'=2] {'sp','tp'}, dimensions={0} | all-to-all | bytes 8388608 | tf_op jit(solution)/shard_map/all_to_all | solution.py:266
  75.3 0.0 copy-done
  75.3 7.9 %expert.1 = (bf16[1024,2048]{1,0:T(8,128)(2,1)S(1)}, f32[128,2048]{1,0:T(8,128)S(1)}) custom-call(bf16[1024,2048]{1,0:T(8,128)(2,1)S(1)} %bitcast.12, bf16[2048,512]{1,0:T(8,128)(2,1)S(1)} %bitcast.15, bf16[2048,512]{1,0:T(8,128)(2,1)S(1)} %bitcast.16, bf16[512,2048]{1,0:T(8,128)(2,1)S(1)} %bitcast.17, bf16[128,2048]{1,0:T(8,128)(2,1)S(1)} %get-tuple-element.33.ffn_ref, ...), custom_call_target="tpu_custom_call" | custom-call | flops 8589934592 | tf_op jit(solution)/shard_map/expert/pallas_call | solution.py:269
  83.3 56.9 %all_to_all.11 = bf16[128,8,2048]{2,1,0:T(8,128)(2,1)S(1)} all-to-all(bf16[128,8,2048]{2,1,0:T(8,128)(2,1)S(1)} %bitcast.13), channel_id=1, replica_groups=mesh['sp'=64,'tp'=2] {'sp','tp'}, dimensions={0} | all-to-all | bytes 8388608 | tf_op jit(solution)/shard_map/all_to_all | solution.py:275
  140.1 1.9 %combine.1 = bf16[128,2048]{1,0:T(8,128)(2,1)} custom-call(bf16[256,1024]{1,0:T(8,128)(2,1)S(1)} %get-tuple-element.21.mix_ref, f32[128,2048]{1,0:T(8,128)S(1)} %get-tuple-element.35.base_ref, bf16[1024,2048]{1,0:T(8,128)(2,1)S(1)} %bitcast.14), custom_call_target="tpu_custom_call" | custom-call | flops 8589934592 | tf_op jit(solution)/shard_map/combine/pallas_call | solution.py:279
  (23 shorter events, 0.1 us)
Async XLA Ops:
  0.0 4.9 %copy-start.15 = (bf16[512]{0:T(512)(128)(2,1)S(1)}, bf16[512]{0:T(512)(128)(2,1)}, u32[]{:S(2)}) copy-start(bf16[512]{0:T(512)(128)(2,1)} %param.23) | copy-start | bytes 3076
  0.0 4.9 %copy-start.7 = (bf16[256,512]{1,0:T(8,128)(2,1)S(1)}, bf16[256,512]{1,0:T(8,128)(2,1)}, u32[]{:S(2)}) copy-start(bf16[256,512]{1,0:T(8,128)(2,1)} %gate_ref.3) | copy-start | bytes 786436
  0.0 4.9 %copy-start.8 = (bf16[256,512]{1,0:T(8,128)(2,1)S(1)}, bf16[256,512]{1,0:T(8,128)(2,1)}, u32[]{:S(2)}) copy-start(bf16[256,512]{1,0:T(8,128)(2,1)} %input_ref.5) | copy-start | bytes 786436
  0.0 4.9 %copy-start.9 = (bf16[256,512]{1,0:T(8,128)(2,1)S(1)}, bf16[256,512]{1,0:T(8,128)(2,1)}, u32[]{:S(2)}) copy-start(bf16[256,512]{1,0:T(8,128)(2,1)} %value_ref.5) | copy-start | bytes 786436
  0.0 4.9 %copy-start.10 = (bf16[3,512]{1,0:T(4,128)(2,1)S(1)}, bf16[3,512]{1,0:T(4,128)(2,1)}, u32[]{:S(2)}) copy-start(bf16[3,512]{1,0:T(4,128)(2,1)} %taps_ref.3) | copy-start | bytes 9220
  0.0 4.9 %copy-start.11 = (s32[128,4]{0,1:T(4,128)S(1)}, s32[128,4]{0,1:T(4,128)}, u32[]{:S(2)}) copy-start(s32[128,4]{0,1:T(4,128)} %param.26) | copy-start | bytes 6148
  0.0 4.9 %copy-start.12 = (f32[128,4]{0,1:T(4,128)S(1)}, f32[128,4]{0,1:T(4,128)}, u32[]{:S(2)}) copy-start(f32[128,4]{0,1:T(4,128)} %param.27) | copy-start | bytes 6148
  0.0 4.9 %copy-start.13 = (s32[256]{0:T(256)S(1)}, s32[256]{0:T(256)}, u32[]{:S(2)}) copy-start(s32[256]{0:T(256)} %param.21) | copy-start | bytes 3076
  0.9 7.3 %collective-permute-start = (bf16[24,512]{1,0:T(8,128)(2,1)S(1)}, bf16[24,512]{1,0:T(8,128)(2,1)S(1)}, u32[]{:S(2)}, u32[]{:S(2)}) collective-permute-start(bf16[24,512]{1,0:T(8,128)(2,1)S(1)} %tail.1), channel_id=1, source_target_pairs={{0,2},{2,4},{4,6},{6,8},{8,10},{10,12},{12,14},{14,16},{16,18},{18... | collective-permute-start | bytes 73736 | tf_op jit(solution)/shard_map/ppermute | solution.py:222
  5.0 3.3 %copy-start.14 = (bf16[2048]{0:T(1024)(128)(2,1)S(1)}, bf16[2048]{0:T(1024)(128)(2,1)}, u32[]{:S(2)}) copy-start(bf16[2048]{0:T(1024)(128)(2,1)} %param.25) | copy-start | bytes 12292
  8.5 2.0 %collective-permute-start.1 = (bf16[128,640]{1,0:T(8,128)(2,1)S(1)}, bf16[128,640]{1,0:T(8,128)(2,1)S(1)}, u32[]{:S(2)}, u32[]{:S(2)}) collective-permute-start(bf16[128,640]{1,0:T(8,128)(2,1)S(1)} %get-tuple-element.28), channel_id=1, source_target_pairs={{0,1},{1,0},{2,3},{3,2},{4,5},{5,4},{6,7},{7,6},{8,9},{9,8},{10,11... | collective-permute-start | bytes 491528 | tf_op jit(solution)/shard_map/ppermute | solution.py:250
  9.5 1.0 copy-start.6
  10.5 64.8 %copy-start.4 = (bf16[2048,512]{1,0:T(8,128)(2,1)S(1)}, bf16[2048,512]{1,0:T(8,128)(2,1)}, u32[]{:S(2)}) copy-start(bf16[2048,512]{1,0:T(8,128)(2,1)} %shared_up_ref.1) | copy-start | bytes 6291460
  10.5 64.8 %copy-start.5 = (bf16[512,2048]{1,0:T(8,128)(2,1)S(1)}, bf16[512,2048]{1,0:T(8,128)(2,1)}, u32[]{:S(2)}) copy-start(bf16[512,2048]{1,0:T(8,128)(2,1)} %shared_down_ref.1) | copy-start | bytes 6291460
  12.4 62.9 %copy-start = (bf16[1,2048,512]{2,1,0:T(8,128)(2,1)S(1)}, bf16[1,2048,512]{2,1,0:T(8,128)(2,1)}, u32[]{:S(2)}) copy-start(bf16[1,2048,512]{2,1,0:T(8,128)(2,1)} %param.31) | copy-start | bytes 6291460
  12.4 62.9 %copy-start.1 = (bf16[1,2048,512]{2,1,0:T(8,128)(2,1)S(1)}, bf16[1,2048,512]{2,1,0:T(8,128)(2,1)}, u32[]{:S(2)}) copy-start(bf16[1,2048,512]{2,1,0:T(8,128)(2,1)} %param.32) | copy-start | bytes 6291460
  12.5 62.9 %copy-start.2 = (bf16[1,512,2048]{2,1,0:T(8,128)(2,1)S(1)}, bf16[1,512,2048]{2,1,0:T(8,128)(2,1)}, u32[]{:S(2)}) copy-start(bf16[1,512,2048]{2,1,0:T(8,128)(2,1)} %param.33) | copy-start | bytes 6291460
  12.5 62.9 %copy-start.3 = (bf16[2048,512]{1,0:T(8,128)(2,1)S(1)}, bf16[2048,512]{1,0:T(8,128)(2,1)}, u32[]{:S(2)}) copy-start(bf16[2048,512]{1,0:T(8,128)(2,1)} %shared_gate_ref.1) | copy-start | bytes 6291460
